TPU v7x, 256 devices: a whole 4x4x8 slice. The times are simulated.
256 devices in a mesh: ep: 128 (over z, y, x), tp: 2 (over core).
Axes of the slice: x: 4, y: 4, z: 8, core: 2. Of those that a mesh axis runs over, the one named last changes fastest.
Arguments:
- inputs: bfloat16 [2048, 1536], P('ep'), may hold values from -6 to 6
- norm_gain_attn: float32 [1536], replicated, may hold values from 0.1 to 1.9
- w_query: bfloat16 [1536, 768], P(None, 'tp'), may hold values from -0.15625 to 0.15625
- w_key: bfloat16 [1536, 128], P(None, 'tp'), may hold values from -0.15625 to 0.15625
- w_value: bfloat16 [1536, 128], P(None, 'tp'), may hold values from -0.15625 to 0.15625
- w_forget: bfloat16 [1536, 12], P(None, 'tp'), may hold values from -0.15625 to 0.15625
- forget_bias: float32 [12], P('tp'), may hold values from 0 to 3
- cache_keys: bfloat16 [2048, 2, 1024, 64], P('ep', 'tp'), may hold values from -250 to 250
- cache_values: bfloat16 [2048, 2, 1024, 64], P('ep', 'tp'), may hold values from -6 to 6
- cache_gates: float32 [2048, 12, 1024], P('ep', 'tp'), as said below
- lengths: int32 [2048], P('ep'), may hold values from 128 to 1024, as said below
- w_out: bfloat16 [768, 1536], P('tp'), may hold values from -0.21875 to 0.21875
- norm_gain_ffn: float32 [1536], replicated, may hold values from 0.1 to 1.9
- expert_ids: int32 [2048, 6], P('ep'), may hold values from 0 to 127, as said below
- group_weights: float32 [2048], P('ep'), may hold values from 0.2 to 1
- expert_weights: float32 [2048, 6], P('ep'), may hold values from 0.05 to 1
- exp_gate: bfloat16 [128, 1536, 512], P('ep', None, 'tp'), may hold values from -0.15625 to 0.15625
- exp_up: bfloat16 [128, 1536, 512], P('ep', None, 'tp'), may hold values from -0.15625 to 0.15625
- exp_down: bfloat16 [128, 512, 1536], P('ep', 'tp'), may hold values from -0.25 to 0.25
- dense_gate_vector: float32 [1536], replicated, may hold values from -0.15625 to 0.15625
- dense_gate_w: bfloat16 [1536, 16384], P(None, ('ep', 'tp')), may hold values from -0.15625 to 0.15625
- dense_up_w: bfloat16 [1536, 16384], P(None, ('ep', 'tp')), may hold values from -0.15625 to 0.15625
- dense_down_w: bfloat16 [16384, 1536], P(('ep', 'tp')), may hold values from -0.09375 to 0.09375
Outputs:
- mixed: bfloat16 [2048, 1536], P('ep', 'tp')
Inputs may be any that keep to these rules, and one draw needn't show every extreme that they name: `cache_gates`: Non-increasing along positions. `lengths`: some sequence has 1024. `expert_ids`: each row names 6 different experts that share one group (the same quotient by 8). Among the rows of one index of ep at most 2 name the same expert, and some expert is named by exactly 2 rows of every index of ep.
All inputs are finite; a program needn't handle non-finite values.
Results may differ from a plain program's by a relative error of at most 0.013.
Values may be sent and summed in bfloat16 or wider, within the bound.
A program may use at most 128 MiB of HBM per device.

v0:
```python
import jax
import jax.numpy as jnp
from jax import lax
from jax.sharding import Mesh
from jax.sharding import PartitionSpec as P

EP = ("ep_0", "ep_1", "ep_2")
EP_TP = ("ep_0", "ep_1", "ep_2", "tp")


EPS = 1e-06


def sent_to_all(value, axis):
    length = lax.axis_size(axis)
    return lax.all_to_all(
        jnp.broadcast_to(value[None], (length, *value.shape)), axis, 0, 0, tiled=True
    )


def of_everyone(value, axis):
    everything = sent_to_all(value, axis)
    return jnp.sum(everything.astype(jnp.float32), axis=0)


def cut_along(value, dim, length):
    before, after = (value.shape[:dim], value.shape[dim + 1 :])
    return jnp.moveaxis(value.reshape(*before, length, -1, *after), dim, 0)


def sent_and_summed(value, axis, dim):
    length = lax.axis_size(axis)
    blocks = lax.all_to_all(cut_along(value, dim, length), axis, 0, 0, tiled=True)
    return jnp.sum(blocks.astype(jnp.float32), axis=0)


def gather_axes(value, axes, dim):
    if not axes:
        return value
    nearer = lax.all_gather(value, axes[-1], axis=dim, tiled=True)
    return gather_axes(nearer, axes[:-1], dim)


def rms_scale(row_block, gain):
    row_block = row_block.astype(jnp.float32)
    factor = lax.rsqrt(jnp.mean(row_block * row_block, axis=-1, keepdims=True) + EPS)
    return (row_block * factor * gain).astype(jnp.bfloat16)


def attend(queries, new_key, new_value, log_forget, keys, values, gates, counts):
    seqs_here, kv_count, group_size, head_size = queries.shape
    cache_positions = lax.broadcasted_iota(jnp.int32, (1, 1, gates.shape[2]), 2)
    last_gate = jnp.sum(
        jnp.where(cache_positions == (counts - 1)[:, None, None], gates, 0.0), axis=2
    )
    offsets = (last_gate + log_forget)[:, :, None] - gates
    offsets = offsets.reshape(seqs_here, kv_count, group_size, gates.shape[2])
    scale_factor = head_size ** (-0.5)
    cached = (
        jnp.einsum("skgd,skld->skgl", queries, keys, preferred_element_type=jnp.float32)
        * scale_factor
        + offsets
    )
    valid_mask = cache_positions.reshape(1, 1, 1, -1) < counts[:, None, None, None]
    cached = jnp.where(valid_mask, cached, -jnp.inf)
    own_score = (
        jnp.einsum("skgd,skd->skg", queries, new_key, preferred_element_type=jnp.float32)
        * scale_factor
    )
    peak_score = jnp.maximum(jnp.max(cached, axis=3), own_score)
    cached_exp = jnp.exp(cached - peak_score[..., None])
    own_exp = jnp.exp(own_score - peak_score)
    denominator = jnp.sum(cached_exp, axis=3) + own_exp
    cached_weight = (cached_exp / denominator[..., None]).astype(jnp.bfloat16)
    own_weight = (own_exp / denominator).astype(jnp.bfloat16)
    mixed_values = jnp.einsum(
        "skgl,skld->skgd", cached_weight, values, preferred_element_type=jnp.float32
    )
    mixed_values = (
        mixed_values
        + own_weight.astype(jnp.float32)[..., None] * new_value.astype(jnp.float32)[:, :, None, :]
    )
    return mixed_values.reshape(seqs_here, kv_count * group_size * head_size).astype(jnp.bfloat16)


def shards(
    inputs,
    norm_gain_attn,
    w_query,
    w_key,
    w_value,
    w_forget,
    forget_bias,
    cache_keys,
    cache_values,
    cache_gates,
    lengths,
    w_out,
    norm_gain_ffn,
    expert_ids,
    group_weights,
    expert_weights,
    exp_gate,
    exp_up,
    exp_down,
    dense_gate_vector,
    dense_gate_w,
    dense_up_w,
    dense_down_w,
):
    seqs_here, model_width = inputs.shape
    kv_count = cache_keys.shape[1]
    head_size = cache_keys.shape[3]
    heads_here = w_forget.shape[1]
    group_size = heads_here // kv_count
    normed = rms_scale(inputs, norm_gain_attn)
    queries = jnp.dot(normed, w_query, preferred_element_type=jnp.float32).astype(jnp.bfloat16)
    queries = queries.reshape(seqs_here, kv_count, group_size, head_size)
    new_key = (
        jnp.dot(normed, w_key, preferred_element_type=jnp.float32)
        .astype(jnp.bfloat16)
        .reshape(seqs_here, kv_count, head_size)
    )
    new_value = (
        jnp.dot(normed, w_value, preferred_element_type=jnp.float32)
        .astype(jnp.bfloat16)
        .reshape(seqs_here, kv_count, head_size)
    )
    log_forget = jax.nn.log_sigmoid(
        jnp.dot(normed, w_forget, preferred_element_type=jnp.float32) + forget_bias
    )
    heads_out = attend(
        queries, new_key, new_value, log_forget, cache_keys, cache_values, cache_gates, lengths
    )
    partial_attn = jnp.dot(heads_out, w_out, preferred_element_type=jnp.float32)
    attn_out = of_everyone(partial_attn.astype(jnp.bfloat16), "tp").astype(jnp.float32)
    after_attn = inputs.astype(jnp.float32) + attn_out
    normed_ffn = rms_scale(after_attn, norm_gain_ffn)
    n_ep = lax.axis_size(EP)
    top_k = expert_ids.shape[1]
    local_experts = exp_gate.shape[0]
    n_experts = n_ep * local_experts
    capacity = max(2, (2 * top_k * seqs_here + n_experts - 1) // n_experts)
    flat_ids = expert_ids.reshape(-1)
    hit_table = (flat_ids[:, None] == lax.broadcasted_iota(jnp.int32, (1, n_experts), 1)).astype(
        jnp.int32
    )
    earlier = jnp.cumsum(hit_table, axis=0) - hit_table
    slot_rank = jnp.sum(earlier * hit_table, axis=1)
    slot_index = flat_ids * capacity + slot_rank
    slot_hits = slot_index[:, None] == lax.broadcasted_iota(jnp.int32, (1, n_experts * capacity), 1)
    repeated = jnp.repeat(normed_ffn, top_k, axis=0)
    outgoing = jnp.einsum(
        "ae,ad->ed", slot_hits.astype(jnp.bfloat16), repeated, preferred_element_type=jnp.float32
    )
    outgoing = outgoing.astype(jnp.bfloat16).reshape(n_ep, local_experts, capacity, model_width)
    arrived = lax.all_to_all(outgoing, EP, split_axis=0, concat_axis=0, tiled=True)
    gate_part = jnp.einsum("secd,edf->secf", arrived, exp_gate, preferred_element_type=jnp.float32)
    up_part = jnp.einsum("secd,edf->secf", arrived, exp_up, preferred_element_type=jnp.float32)
    activated = (jax.nn.silu(gate_part) * up_part).astype(jnp.bfloat16)
    partial_out = jnp.einsum(
        "secf,efd->secd", activated, exp_down, preferred_element_type=jnp.float32
    )
    summed = sent_and_summed(partial_out.astype(jnp.bfloat16), "tp", 3)
    returned = lax.all_to_all(
        summed.astype(jnp.bfloat16), EP, split_axis=0, concat_axis=0, tiled=True
    )
    half_width = returned.shape[3]
    route_weight = (group_weights[:, None] * expert_weights).reshape(-1, 1)
    combine = (slot_hits.astype(jnp.float32) * route_weight).reshape(
        seqs_here, top_k, n_experts * capacity
    )
    combine = jnp.sum(combine, axis=1)
    expert_mix = jnp.dot(
        combine,
        returned.reshape(n_experts * capacity, half_width).astype(jnp.float32),
        precision=lax.Precision.HIGHEST,
    )
    gating = jax.nn.sigmoid(
        jnp.dot(normed_ffn.astype(jnp.float32), dense_gate_vector, precision=lax.Precision.HIGHEST)
    )
    all_rows = gather_axes(normed_ffn, EP, 0)
    gate_part = jnp.dot(all_rows, dense_gate_w, preferred_element_type=jnp.float32)
    up_part = jnp.dot(all_rows, dense_up_w, preferred_element_type=jnp.float32)
    activated = (jax.nn.silu(gate_part) * up_part).astype(jnp.bfloat16)
    shares = lax.psum_scatter(
        jnp.dot(activated, dense_down_w, preferred_element_type=jnp.float32).astype(jnp.bfloat16),
        EP_TP,
        scatter_dimension=0,
        tiled=True,
    ).astype(jnp.float32)
    dense_out = lax.all_to_all(
        shares.astype(jnp.bfloat16), "tp", split_axis=1, concat_axis=0, tiled=True
    ).astype(shares.dtype)
    own_cols = lax.dynamic_slice_in_dim(
        after_attn, lax.axis_index("tp") * half_width, half_width, 1
    )
    return (own_cols + expert_mix + gating[:, None] * dense_out).astype(jnp.bfloat16)


def solution(mesh):
    torus = Mesh(mesh.devices.reshape(8, 4, 4, mesh.shape["tp"]), ("ep_0", "ep_1", "ep_2", "tp"))
    placed = (
        P(EP, None),
        P(),
        P(None, "tp"),
        P(None, "tp"),
        P(None, "tp"),
        P(None, "tp"),
        P("tp"),
        P(EP, "tp", None, None),
        P(EP, "tp", None, None),
        P(EP, "tp", None),
        P(EP),
        P("tp", None),
        P(),
        P(EP, None),
        P(EP),
        P(EP, None),
        P(EP, None, "tp"),
        P(EP, None, "tp"),
        P(EP, "tp", None),
        P(),
        P(None, EP_TP),
        P(None, EP_TP),
        P(EP_TP, None),
    )
    return jax.shard_map(
        shards, mesh=torus, in_specs=placed, out_specs=P(EP, "tp"), check_vma=False
    )
```

profile of v0, /device:TPU:1, one launch (start us, length us, event | category | flops | bytes accessed | tf_op | source)
XLA Modules:
  0.0 552.1 jit_solution(2104474610702420346)
XLA Ops:
  6.5 0.8 broadcast_add_fusion
  7.3 0.7 iota_compare_fusion.4
  8.1 0.9 fusion.59
  9.0 1.6 convolution_convert_fusion.4
  10.7 0.1 reshape.198
  10.8 0.1 iota_compare_fusion.3
  10.9 1.1 select_reduce_fusion
  12.0 1.0 fusion.68
  13.0 0.0 copy-start.3
  13.0 0.0 copy-start.8
  13.0 0.1 copy.56
  13.1 1.2 fusion.26
  14.3 0.1 fusion.64
  14.5 0.6 fusion.76
  15.1 0.2 fusion.49
  15.4 0.2 fusion.25
  15.6 0.3 copy-done.13
  15.9 0.7 fusion.20
  16.6 0.1 convert_element_type.104
  16.8 0.3 convolution_convert_fusion.3
  17.0 6.8 %all_to_all.33 = bf16[2,16,1536]{2,1,0:T(8,128)(2,1)S(1)} all-to-all(bf16[2,16,1536]{2,1,0:T(8,128)(2,1)S(1)} %broadcast_in_dim.32), channel_id=1, replica_groups=mesh['ep_0'=8,'ep_1'=4,'ep_2'=4,'tp'=2] {'tp'}, dimensions={0} | all-to-all | bytes 196608 | tf_op jit(solution)/shard_map/all_to_all | solution.py:16
  23.8 0.1 multiply_reduce_fusion
  24.0 0.1 multiply_convert_fusion
  24.1 9.2 %all_gather.9 = bf16[64,1536]{1,0:T(8,128)(2,1)S(1)} all-gather(bf16[16,1536]{1,0:T(8,128)(2,1)S(1)} %multiply_convert_fusion), channel_id=1, replica_groups=mesh['ep_0'=8,'ep_1'=4,'ep_2'=4,'tp'=2] {'ep_2'}, dimensions={0}, use_global_device_ids=true | all-gather | bytes 245760 | tf_op jit(solution)/shard_map/all_gather | solution.py:40
  33.3 11.6 %all_gather.10 = bf16[256,1536]{1,0:T(8,128)(2,1)} all-gather(bf16[64,1536]{1,0:T(8,128)(2,1)S(1)} %all_gather.9), channel_id=1, replica_groups=mesh['ep_0'=8,'ep_1'=4,'ep_2'=4,'tp'=2] {'ep_1'}, dimensions={0}, use_global_device_ids=true | all-gather | bytes 983040 | tf_op jit(solution)/shard_map/all_gather | solution.py:40
  44.9 0.0 all-gather.2.cloned.1.call-update
  45.0 0.0 copy-start.5
  45.0 0.0 copy-start.6
  45.0 0.0 reduce-scatter.2.cloned.1.call-start
  45.0 80.3 %all-gather.2.cloned.1.call-done = bf16[2048,1536]{1,0:T(8,128)(2,1)} async-done(((bf16[256,1536]{1,0:T(8,128)(2,1)}), bf16[2048,1536]{1,0:T(8,128)(2,1)}) %all-gather.2.cloned.1.call-update) | async-done | bytes 6291472 | tf_op jit(solution)/shard_map/all_gather | solution.py:40
  125.3 4.8 fusion.77
  130.1 10.2 %convolution_convert_fusion = bf16[2048,1536]{1,0:T(8,128)(2,1)} fusion(bf16[64,1536]{1,0:T(8,128)(2,1)S(1)} %copy-done.5, bf16[2048,1536]{1,0:T(8,128)(2,1)} %all-gather.2.cloned.1.call-done, bf16[1536,64]{0,1:T(8,128)(2,1)S(1)} %copy-done.6, f32[2048,64]{0,1:T(8,128)S(1)} %fusion.77), kind=kOutput, calls=%fused_computation | convolution fusion | flops 809238528 | bytes 13500416 | tf_op jit(solution)/shard_map/dot_general | solution.py:187
  140.4 0.0 reduce-scatter.2.cloned.1.call-update
  140.4 0.1 reshape.201
  140.6 0.5 copy-done.7
  141.1 0.1 copy.58
  141.1 0.1 eq.56
  141.2 0.1 fusion.63
  141.3 0.1 reduce_window_sum.11
  141.5 0.2 select_reduce_fusion.2
  141.6 0.0 copy-start.10
  141.7 0.5 convolution_convert_fusion.2
  142.1 1.2 reshape.202
  143.3 11.1 %all-to-all-start.1 = ((bf16[128,1,2,1536]{3,2,1,0:T(2,128)(2,1)}), bf16[128,1,2,1536]{3,2,1,0:T(2,128)(2,1)S(1)}, u32[]{:S(2)}, u32[]{:S(2)}) async-start(bf16[128,1,2,1536]{3,2,1,0:T(2,128)(2,1)} %bitcast.5), calls=%async_computation.1 | async-start | bytes 1572864 | tf_op jit(solution)/shard_map/all_to_all | solution.py:157
  154.5 0.1 reduce_sum.84
  154.5 0.0 copy-done.10
  154.6 0.1 copy.59
  154.7 23.4 %all-to-all-done.1 = bf16[128,1,2,1536]{3,2,1,0:T(2,128)(2,1)S(1)} async-done(((bf16[128,1,2,1536]{3,2,1,0:T(2,128)(2,1)}), bf16[128,1,2,1536]{3,2,1,0:T(2,128)(2,1)S(1)}, u32[]{:S(2)}, u32[]{:S(2)}) %all-to-all-start.1) | async-done | bytes 786464 | tf_op jit(solution)/shard_map/all_to_all | solution.py:157
  178.0 1.5 convolution_bitcast_fusion.1
  179.6 3.3 convolution_convert_fusion.1
  182.9 1.2 copy.84
  184.1 0.0 copy-start.11
  184.1 0.0 copy-start.12
  184.1 7.5 %all_to_all.34 = bf16[2,128,1,2,768]{4,1,3,2,0:T(8,128)(2,1)S(1)} all-to-all(bf16[2,128,1,2,768]{4,1,3,2,0:T(8,128)(2,1)S(1)} %bitcast.116), channel_id=1, replica_groups=mesh['ep_0'=8,'ep_1'=4,'ep_2'=4,'tp'=2] {'tp'}, dimensions={0} | all-to-all | bytes 1572864 | tf_op jit(solution)/shard_map/all_to_all | solution.py:33
  191.6 0.1 reduce_sum.87
  191.7 1.2 copy.64
  192.9 6.2 %all-to-all-start.3 = ((bf16[128,1,2,768]{3,2,1,0:T(2,128)(2,1)}), bf16[128,1,2,768]{3,2,1,0:T(2,128)(2,1)S(1)}, u32[]{:S(2)}, u32[]{:S(2)}) async-start(bf16[128,1,2,768]{3,2,1,0:T(2,128)(2,1)} %copy.64), calls=%async_computation.3 | async-start | bytes 786432 | tf_op jit(solution)/shard_map/all_to_all | solution.py:165
  199.1 0.1 select_reduce_fusion.1
  199.2 0.1 fusion.31
  199.3 16.3 %all-to-all-done.3 = bf16[128,1,2,768]{3,2,1,0:T(2,128)(2,1)S(1)} async-done(((bf16[128,1,2,768]{3,2,1,0:T(2,128)(2,1)}), bf16[128,1,2,768]{3,2,1,0:T(2,128)(2,1)S(1)}, u32[]{:S(2)}, u32[]{:S(2)}) %all-to-all-start.3) | async-done | bytes 393248 | tf_op jit(solution)/shard_map/all_to_all | solution.py:165
  215.6 0.1 reshape.209
  215.8 318.9 %reduce-scatter.2.cloned.1.call-done = bf16[8,1536]{1,0:T(8,128)(2,1)} async-done(((bf16[2048,1536]{1,0:T(8,128)(2,1)}), bf16[8,1536]{1,0:T(8,128)(2,1)}) %reduce-scatter.2.cloned.1.call-update) | async-done | bytes 24592 | tf_op jit(solution)/shard_map/reduce_scatter | solution.py:186
  534.7 9.7 %all_to_all.35 = bf16[8,2,768]{2,0,1:T(8,128)(2,1)S(1)} all-to-all(bf16[8,2,768]{2,0,1:T(8,128)(2,1)} %bitcast.121), channel_id=1, replica_groups=mesh['ep_0'=8,'ep_1'=4,'ep_2'=4,'tp'=2] {'tp'}, dimensions={1} | all-to-all | bytes 49152 | tf_op jit(solution)/shard_map/all_to_all | solution.py:192
  544.4 0.9 fusion.24
  (32 shorter events, 0.2 us)
Async XLA Ops:
  6.5 7.9 %copy-start = (bf16[16,1,1024,64]{2,3,1,0:T(8,128)(2,1)S(1)}, bf16[16,1,1024,64]{2,3,1,0:T(8,128)(2,1)}, u32[]{:S(2)}) copy-start(bf16[16,1,1024,64]{2,3,1,0:T(8,128)(2,1)} %param.30) | copy-start | bytes 6291460
  6.5 7.9 %copy-start.1 = (f32[16,6,1024]{2,0,1:T(8,128)S(1)}, f32[16,6,1024]{2,0,1:T(8,128)}, u32[]{:S(2)}) copy-start(f32[16,6,1024]{2,0,1:T(8,128)} %param.32) | copy-start | bytes 1179652
  6.5 118.8 %all-gather.2.cloned.1.call-start = ((), (), s32[]{:S(2)}) async-start(), calls=%async_computation.6 | async-start | bytes 7077888 | tf_op jit(solution)/shard_map/all_gather | solution.py:40
  13.0 2.4 copy-start.3
  13.0 2.4 copy-start.8
  13.1 2.3 copy-start.14
  14.3 1.6 copy-start.13
  15.1 1.7 copy-start.2
  15.9 8.1 %copy-start.9 = (f32[1536]{0:T(1024)S(1)}, f32[1536]{0:T(1024)}, u32[]{:S(2)}) copy-start(f32[1536]{0:T(1024)} %param.35) | copy-start | bytes 18436
  17.0 108.3 %copy-start.4 = (bf16[1536,64]{0,1:T(8,128)(2,1)S(1)}, bf16[1536,64]{0,1:T(8,128)(2,1)}, u32[]{:S(2)}) copy-start(bf16[1536,64]{0,1:T(8,128)(2,1)} %param.43) | copy-start | bytes 589828
  45.0 85.1 %copy-start.5 = (bf16[64,1536]{1,0:T(8,128)(2,1)S(1)}, bf16[64,1536]{1,0:T(8,128)(2,1)}, u32[]{:S(2)}) copy-start(bf16[64,1536]{1,0:T(8,128)(2,1)} %param.45) | copy-start | bytes 589828
  45.0 85.1 %copy-start.6 = (bf16[1536,64]{0,1:T(8,128)(2,1)S(1)}, bf16[1536,64]{0,1:T(8,128)(2,1)}, u32[]{:S(2)}) copy-start(bf16[1536,64]{0,1:T(8,128)(2,1)} %param.44) | copy-start | bytes 589828
  45.0 489.7 %reduce-scatter.2.cloned.1.call-start = ((), (), s32[]{:S(2)}) async-start(), calls=%async_computation.7 | async-start | bytes 6316032 | tf_op jit(solution)/shard_map/reduce_scatter | solution.py:186
  140.4 0.7 copy-start.7
  141.6 12.9 %copy-start.10 = (f32[1536]{0:T(1024)S(1)}, f32[1536]{0:T(1024)}, u32[]{:S(2)}) copy-start(f32[1536]{0:T(1024)} %param.42) | copy-start | bytes 18436
  143.3 34.7 %all-to-all-start.1 = ((bf16[128,1,2,1536]{3,2,1,0:T(2,128)(2,1)}), bf16[128,1,2,1536]{3,2,1,0:T(2,128)(2,1)S(1)}, u32[]{:S(2)}, u32[]{:S(2)}) async-start(bf16[128,1,2,1536]{3,2,1,0:T(2,128)(2,1)} %bitcast.5), calls=%async_computation.1 | async-start | bytes 1572864 | tf_op jit(solution)/shard_map/all_to_all | solution.py:157
  184.1 15.0 %copy-start.11 = (f32[16,6]{0,1:T(8,128)S(1)}, f32[16,6]{0,1:T(8,128)}, u32[]{:S(2)}) copy-start(f32[16,6]{0,1:T(8,128)} %param.38) | copy-start | bytes 1156
  184.1 15.0 %copy-start.12 = (f32[16]{0:T(128)S(1)}, f32[16]{0:T(128)}, u32[]{:S(2)}) copy-start(f32[16]{0:T(128)} %param.37) | copy-start | bytes 196
  192.9 22.7 %all-to-all-start.3 = ((bf16[128,1,2,768]{3,2,1,0:T(2,128)(2,1)}), bf16[128,1,2,768]{3,2,1,0:T(2,128)(2,1)S(1)}, u32[]{:S(2)}, u32[]{:S(2)}) async-start(bf16[128,1,2,768]{3,2,1,0:T(2,128)(2,1)} %copy.64), calls=%async_computation.3 | async-start | bytes 786432 | tf_op jit(solution)/shard_map/all_to_all | solution.py:165
Sparse Core Ops, SparseCore 0:
  45.1 80.1 all-gather.1
  140.5 394.1 reduce-scatter.1
where the time goes:
time: 553 us; the launch traced here: 552 us
  waiting for transfers between devices  439 us (79%)
  blocking collectives  44.9 us (8%)
  matrix products  27.1 us (5%)
  starting transfers between devices  17.4 us (3%)
  between operations  13.7 us (2%)
    reduce_scatter x1, waiting for transfers between devices, shards(): lax.psum_scatter(jnp.dot(activated, dense_down_w, preferred_element_type=...  319 us
    all_gather x1, waiting for transfers between devices, gather_axes(): nearer = lax.all_gather(value, axes[-1], axis=dim, tiled=True)  80.3 us
    all_to_all x1, waiting for transfers between devices, shards(): lax.all_to_all(outgoing, EP, split_axis=0, concat_axis=0, tiled=True)  23.4 us
    all_gather x2, blocking collectives, gather_axes(): nearer = lax.all_gather(value, axes[-1], axis=dim, tiled=True)  20.9 us
    all_to_all x1, waiting for transfers between devices, shards(): lax.all_to_all(summed.astype(jnp.bfloat16), EP, split_axis=0, concat_axis...  16.3 us
    all_to_all x1, starting transfers between devices, shards(): lax.all_to_all(outgoing, EP, split_axis=0, concat_axis=0, tiled=True)  11.1 us
  transfers between devices with their start and end apart: 4, of which 4 were waited for; matrix products, arithmetic and copies ran while one was open for 2% of the time, Pallas kernels for 0%

commit v1 on v0

v1 whole, which is shorter than its diff:
```python
import jax
import jax.numpy as jnp
from jax import lax
from jax.experimental import pallas as pl
from jax.experimental.pallas import tpu as pltpu
from jax.sharding import Mesh
from jax.sharding import PartitionSpec as P

EP = ("ep_0", "ep_1", "ep_2")
EP_TP = ("ep_0", "ep_1", "ep_2", "tp")


EPS = 1e-06


MESH = pl.DeviceIdType.MESH
WIDTH = 1536
HALF = WIDTH // 2
EXTRA = 128
ROW = WIDTH + EXTRA
ROWS = 16

K_PA = 0
K_ZG = 1
K_AU = 9
K_AV = 15
K_PUSH = 21
K_PART = 25
K_RV = 29
K_RU = 35
K_ZR = 41
N_SEM = 49


def mod4(value):
    return lax.rem(value + 8, 4)


def silu(value):
    return value / (1.0 + jnp.exp(-value))


def layer_kernel(
    pa_ref,
    inp_ref,
    gain_ref,
    route_ref,
    wg_ref,
    wu_ref,
    wd_ref,
    ed_ref,
    dd_ref,
    out_ref,
    pr,
    aa,
    xs,
    po,
    dr,
    va,
    vb,
    vf,
    sv,
    ua,
    ub,
    uf,
    su,
    zr,
    ssem,
    rsem,
):
    z = lax.axis_index("ep_0")
    y = lax.axis_index("ep_1")
    x = lax.axis_index("ep_2")
    t = lax.axis_index("tp")
    expert = (z * 4 + y) * 4 + x
    u = (1 - t) * y + t * x
    v = (1 - t) * x + t * y
    part = z // 4
    zz_own = lax.rem(z, 4)

    def near(du, dv):
        return (z, mod4(y + (1 - t) * du + t * dv), mod4(x + (1 - t) * dv + t * du), t)

    partner = (z, y, x, 1 - t)
    u_plus, u_minus = near(1, 0), near(-1, 0)
    v_plus, v_minus = near(0, 1), near(0, -1)

    def send(src, dst, k, device, kr=None):
        copy = pltpu.make_async_remote_copy(
            src_ref=src,
            dst_ref=dst,
            send_sem=ssem.at[k],
            recv_sem=rsem.at[k if kr is None else kr],
            device_id=device,
            device_id_type=MESH,
        )
        copy.start()
        return copy

    def landed(dst, k):
        pltpu.make_async_remote_copy(
            src_ref=dst,
            dst_ref=dst,
            send_sem=ssem.at[k],
            recv_sem=rsem.at[k],
            device_id=partner,
            device_id_type=MESH,
        ).wait_recv()

    barrier = pltpu.get_barrier_semaphore()
    for device in (partner, u_plus, u_minus, v_plus, v_minus):
        pl.semaphore_signal(barrier, inc=1, device_id=device, device_id_type=MESH)
    for dz in range(1, 8):
        for core in range(2):
            pl.semaphore_signal(
                barrier, inc=1, device_id=(lax.rem(z + dz, 8), y, x, core), device_id_type=MESH
            )
    pl.semaphore_wait(barrier, 19)

    sent = []

    sent.append(send(pa_ref, pr, K_PA, partner))
    landed(pr, K_PA)
    attn = pa_ref[...].astype(jnp.float32) + pr[...].astype(jnp.float32)
    after = inp_ref[...].astype(jnp.float32) + attn
    aa[...] = after
    factor = lax.rsqrt(jnp.mean(after * after, axis=-1, keepdims=True) + EPS)
    normed = (after * factor * gain_ref[...]).astype(jnp.bfloat16)

    @pl.when(part == t)
    def _():
        xs[0, v, zz_own, u, :, :WIDTH] = normed
        xs[0, v, zz_own, u, :, WIDTH:] = route_ref[...]
        block = xs.at[0, v, zz_own, u]
        for dz in (4, 3, 5, 2, 6, 1, 7):
            send(block, block, K_ZG + dz, (lax.rem(z + dz, 8), y, x, t), K_ZG + zz_own)

    for zz in range(4):

        @pl.when(4 * t + zz != z)
        def _():
            landed(xs.at[0, v, zz, u], K_ZG + zz)

    def ring_gather(piece, w, plus, minus, k):
        own_a, own_b = piece(0, w), piece(1, w)
        sent.append(send(own_a, own_a, k, plus))
        sent.append(send(own_b, own_b, k + 2, minus))
        sent.append(send(own_b, own_b, k + 1, plus))
        sent.append(send(own_a, own_a, k + 3, minus))

    def ring_relay(piece, w, plus, minus, k):
        a_left, b_right = piece(0, mod4(w - 1)), piece(1, mod4(w + 1))
        landed(a_left, k)
        sent.append(send(a_left, a_left, k + 4, plus))
        landed(b_right, k + 2)
        sent.append(send(b_right, b_right, k + 5, minus))

    def piece_u(half, w):
        return xs.at[0, v, pl.ds(2 * half, 2), w]

    def piece_v(half, w):
        return xs.at[0, w, pl.ds(2 * half, 2)]

    ring_gather(piece_u, u, u_plus, u_minus, K_AU)
    ring_relay(piece_u, u, u_plus, u_minus, K_AU)
    landed(piece_u(1, mod4(u - 1)), K_AU + 1)
    landed(piece_u(0, mod4(u + 1)), K_AU + 3)
    landed(piece_u(0, mod4(u + 2)), K_AU + 4)
    landed(piece_u(1, mod4(u + 2)), K_AU + 5)

    ring_gather(piece_v, v, v_plus, v_minus, K_AV)

    def push(w, slot):
        sent.append(send(xs.at[0, w], xs.at[1, w], K_PUSH + slot, partner))

    push(v, 0)

    lane = lax.broadcasted_iota(jnp.int32, (1, EXTRA), 1)

    def unit(side, w):
        rows = xs[side, w].reshape(16 * ROWS, ROW)
        tokens = rows[:, :WIDTH]
        weight = jnp.sum(
            jnp.where(lane == expert, rows[:, WIDTH:].astype(jnp.float32), 0.0),
            axis=1,
            keepdims=True,
        )
        gate = jnp.dot(tokens, wg_ref[...], preferred_element_type=jnp.float32)
        up = jnp.dot(tokens, wu_ref[...], preferred_element_type=jnp.float32)
        hidden = (silu(gate) * up * weight).astype(jnp.bfloat16)
        both = jnp.dot(tokens, wd_ref[...], preferred_element_type=jnp.float32)
        second = both[:, EXTRA:]
        logit = jnp.sum(
            jnp.where((lane >= 64) & (lane < 67), second, 0.0), axis=1, keepdims=True
        )
        gating = 1.0 / (1.0 + jnp.exp(-logit))
        dense = (silu(both[:, :EXTRA]) * second * gating).astype(jnp.bfloat16)
        total = jnp.dot(hidden, ed_ref[...], preferred_element_type=jnp.float32)
        total = total + jnp.dot(dense[:, :64], dd_ref[...], preferred_element_type=jnp.float32)
        po[side, w] = total.astype(jnp.bfloat16).reshape(4, 4, ROWS, WIDTH)

    def give(w, slot):
        sent.append(send(po.at[1, w], dr.at[w], K_PART + slot, partner))

    def received(w, slot):
        landed(xs.at[1, w], K_PUSH + slot)

    unit(0, v)
    received(u, 0)
    unit(1, u)
    give(u, 0)

    ring_relay(piece_v, v, v_plus, v_minus, K_AV)
    landed(piece_v(1, mod4(v - 1)), K_AV + 1)
    push(mod4(v - 1), 1)
    landed(piece_v(0, mod4(v + 1)), K_AV + 3)
    push(mod4(v + 1), 2)
    received(mod4(u - 1), 1)
    received(mod4(u + 1), 2)

    def middle(i, carry):
        side = i // 2
        w = mod4((1 - side) * v + side * u + 2 * lax.rem(i, 2) - 1)
        unit(side, w)
        return carry

    lax.fori_loop(0, 4, middle, 0)
    give(mod4(u - 1), 1)
    give(mod4(u + 1), 2)

    landed(piece_v(0, mod4(v + 2)), K_AV + 4)
    landed(piece_v(1, mod4(v + 2)), K_AV + 5)
    push(mod4(v + 2), 3)
    received(mod4(u + 2), 3)

    def last(i, carry):
        side = 1 - i
        unit(side, mod4((1 - side) * v + side * u + 2))
        return carry

    lax.fori_loop(0, 2, last, 0)
    give(mod4(u + 2), 3)

    f32 = jnp.float32
    bf16 = jnp.bfloat16

    def add_partner(w, slot):
        landed(dr.at[w], K_PART + slot)

        def body(i, carry):
            zz, uu = i // 4, lax.rem(i, 4)
            both = po[0, w, zz, uu].astype(f32) + dr[w, zz, uu].astype(f32)
            po[0, w, zz, uu] = both.astype(bf16)
            return carry

        lax.fori_loop(0, 16, body, 0)

    right, left, far = mod4(v + 1), mod4(v - 1), mod4(v + 2)
    low, high = pl.ds(0, 2), pl.ds(2, 2)
    add_partner(far, 3)
    sent.append(send(po.at[0, far, low], va, K_RV, v_plus))
    sent.append(send(po.at[0, far, high], vb, K_RV + 1, v_minus))
    add_partner(right, 2)
    sent.append(send(po.at[0, right, high], vf.at[1], K_RV + 2, v_plus))
    add_partner(left, 1)
    sent.append(send(po.at[0, left, low], vf.at[0], K_RV + 3, v_minus))
    add_partner(v, 0)

    landed(va, K_RV)

    def add_a(i, carry):
        zz, uu = i // 4, lax.rem(i, 4)
        po[0, right, zz, uu] = (
            po[0, right, zz, uu].astype(f32) + va[zz, uu].astype(f32)
        ).astype(bf16)
        return carry

    lax.fori_loop(0, 8, add_a, 0)
    sent.append(send(po.at[0, right, low], vf.at[2], K_RV + 4, v_plus))
    landed(vb, K_RV + 1)

    def add_b(i, carry):
        zz, uu = i // 4, lax.rem(i, 4)
        po[0, left, 2 + zz, uu] = (
            po[0, left, 2 + zz, uu].astype(f32) + vb[zz, uu].astype(f32)
        ).astype(bf16)
        return carry

    lax.fori_loop(0, 8, add_b, 0)
    sent.append(send(po.at[0, left, high], vf.at[3], K_RV + 5, v_minus))
    landed(vf.at[0], K_RV + 3)
    landed(vf.at[1], K_RV + 2)
    landed(vf.at[2], K_RV + 4)
    landed(vf.at[3], K_RV + 5)

    def add_v(i, carry):
        zz, uu = i // 4, lax.rem(i, 4)
        half, inner = zz // 2, lax.rem(zz, 2)
        total = (
            po[0, v, zz, uu].astype(f32)
            + vf[half, inner, uu].astype(f32)
            + vf[2 + half, inner, uu].astype(f32)
        )
        sv[uu, zz] = total.astype(bf16)
        return carry

    lax.fori_loop(0, 16, add_v, 0)

    right, left, far = mod4(u + 1), mod4(u - 1), mod4(u + 2)
    sent.append(send(sv.at[far, low], ua, K_RU, u_plus))
    sent.append(send(sv.at[far, high], ub, K_RU + 1, u_minus))
    sent.append(send(sv.at[right, high], uf.at[1], K_RU + 2, u_plus))
    sent.append(send(sv.at[left, low], uf.at[0], K_RU + 3, u_minus))
    landed(ua, K_RU)
    for zz in range(2):
        sv[right, zz] = (sv[right, zz].astype(f32) + ua[zz].astype(f32)).astype(bf16)
    sent.append(send(sv.at[right, low], uf.at[2], K_RU + 4, u_plus))
    landed(ub, K_RU + 1)
    for zz in range(2):
        sv[left, 2 + zz] = (sv[left, 2 + zz].astype(f32) + ub[zz].astype(f32)).astype(bf16)
    sent.append(send(sv.at[left, high], uf.at[3], K_RU + 5, u_minus))
    landed(uf.at[0], K_RU + 3)
    landed(uf.at[1], K_RU + 2)
    landed(uf.at[2], K_RU + 4)
    landed(uf.at[3], K_RU + 5)
    for zz in range(4):
        half, inner = zz // 2, zz % 2
        total = (
            sv[u, zz].astype(f32)
            + uf[half, inner].astype(f32)
            + uf[2 + half, inner].astype(f32)
        ).astype(bf16)
        for h in range(2):
            su[zz, h] = total[:, h * HALF : (h + 1) * HALF]

    for zz in range(4):
        for h in range(2):
            here = (4 * t + zz == z) & (t == h)

            @pl.when(jnp.logical_not(here))
            def _():
                send(
                    su.at[zz, h], zr.at[z], K_ZR + zz * 2 + h, (4 * t + zz, y, x, h), K_ZR + z
                )

            @pl.when(here)
            def _():
                zr[z] = su[zz, h]

    for s in range(8):

        @pl.when(jnp.logical_not((z == s) & (part == t)))
        def _():
            landed(zr.at[s], K_ZR + s)

    total = aa[:, pl.ds(pl.multiple_of(t * HALF, HALF), HALF)]
    for s in range(8):
        total = total + zr[s].astype(f32)
    out_ref[...] = total.astype(bf16)

    for copy in sent:
        copy.wait_send()

    def sent_out(src, k):
        pltpu.make_async_remote_copy(
            src_ref=src,
            dst_ref=src,
            send_sem=ssem.at[k],
            recv_sem=rsem.at[k],
            device_id=partner,
            device_id_type=MESH,
        ).wait_send()

    @pl.when(part == t)
    def _():
        for dz in range(1, 8):
            sent_out(xs.at[0, v, zz_own, u], K_ZG + dz)

    for zz in range(4):
        for h in range(2):

            @pl.when(jnp.logical_not((4 * t + zz == z) & (t == h)))
            def _():
                sent_out(su.at[zz, h], K_ZR + zz * 2 + h)


def run_layer(pa, inputs, gain, route, wg, wu, wd, ed, dd):
    bf16 = jnp.bfloat16
    vmem = pl.BlockSpec(memory_space=pltpu.VMEM)
    return pl.pallas_call(
        layer_kernel,
        out_shape=jax.ShapeDtypeStruct((ROWS, HALF), bf16),
        in_specs=[vmem] * 9,
        out_specs=vmem,
        scratch_shapes=[
            pltpu.VMEM((ROWS, WIDTH), bf16),
            pltpu.VMEM((ROWS, WIDTH), jnp.float32),
            pltpu.VMEM((2, 4, 4, 4, ROWS, ROW), bf16),
            pltpu.VMEM((2, 4, 4, 4, ROWS, WIDTH), bf16),
            pltpu.VMEM((4, 4, 4, ROWS, WIDTH), bf16),
            pltpu.VMEM((2, 4, ROWS, WIDTH), bf16),
            pltpu.VMEM((2, 4, ROWS, WIDTH), bf16),
            pltpu.VMEM((4, 2, 4, ROWS, WIDTH), bf16),
            pltpu.VMEM((4, 4, ROWS, WIDTH), bf16),
            pltpu.VMEM((2, ROWS, WIDTH), bf16),
            pltpu.VMEM((2, ROWS, WIDTH), bf16),
            pltpu.VMEM((4, 2, ROWS, WIDTH), bf16),
            pltpu.VMEM((4, 2, ROWS, HALF), bf16),
            pltpu.VMEM((8, ROWS, HALF), bf16),
            pltpu.SemaphoreType.DMA((N_SEM,)),
            pltpu.SemaphoreType.DMA((N_SEM,)),
        ],
        compiler_params=pltpu.CompilerParams(
            collective_id=0, has_side_effects=True, vmem_limit_bytes=52 * 1024 * 1024
        ),
        name="layer",
    )(pa, inputs, gain, route, wg, wu, wd, ed, dd)


def rms_scale(row_block, gain):
    row_block = row_block.astype(jnp.float32)
    factor = lax.rsqrt(jnp.mean(row_block * row_block, axis=-1, keepdims=True) + EPS)
    return (row_block * factor * gain).astype(jnp.bfloat16)


def attend(queries, new_key, new_value, log_forget, keys, values, gates, counts):
    seqs_here, kv_count, group_size, head_size = queries.shape
    cache_positions = lax.broadcasted_iota(jnp.int32, (1, 1, gates.shape[2]), 2)
    last_gate = jnp.sum(
        jnp.where(cache_positions == (counts - 1)[:, None, None], gates, 0.0), axis=2
    )
    offsets = (last_gate + log_forget)[:, :, None] - gates
    offsets = offsets.reshape(seqs_here, kv_count, group_size, gates.shape[2])
    scale_factor = head_size ** (-0.5)
    cached = (
        jnp.einsum("skgd,skld->skgl", queries, keys, preferred_element_type=jnp.float32)
        * scale_factor
        + offsets
    )
    valid_mask = cache_positions.reshape(1, 1, 1, -1) < counts[:, None, None, None]
    cached = jnp.where(valid_mask, cached, -jnp.inf)
    own_score = (
        jnp.einsum("skgd,skd->skg", queries, new_key, preferred_element_type=jnp.float32)
        * scale_factor
    )
    peak_score = jnp.maximum(jnp.max(cached, axis=3), own_score)
    cached_exp = jnp.exp(cached - peak_score[..., None])
    own_exp = jnp.exp(own_score - peak_score)
    denominator = jnp.sum(cached_exp, axis=3) + own_exp
    cached_weight = (cached_exp / denominator[..., None]).astype(jnp.bfloat16)
    own_weight = (own_exp / denominator).astype(jnp.bfloat16)
    mixed_values = jnp.einsum(
        "skgl,skld->skgd", cached_weight, values, preferred_element_type=jnp.float32
    )
    mixed_values = (
        mixed_values
        + own_weight.astype(jnp.float32)[..., None] * new_value.astype(jnp.float32)[:, :, None, :]
    )
    return mixed_values.reshape(seqs_here, kv_count * group_size * head_size).astype(jnp.bfloat16)


def shards(
    inputs,
    norm_gain_attn,
    w_query,
    w_key,
    w_value,
    w_forget,
    forget_bias,
    cache_keys,
    cache_values,
    cache_gates,
    lengths,
    w_out,
    norm_gain_ffn,
    expert_ids,
    group_weights,
    expert_weights,
    exp_gate,
    exp_up,
    exp_down,
    dense_gate_vector,
    dense_gate_w,
    dense_up_w,
    dense_down_w,
):
    seqs_here, model_width = inputs.shape
    kv_count = cache_keys.shape[1]
    head_size = cache_keys.shape[3]
    heads_here = w_forget.shape[1]
    group_size = heads_here // kv_count
    normed = rms_scale(inputs, norm_gain_attn)
    queries = jnp.dot(normed, w_query, preferred_element_type=jnp.float32).astype(jnp.bfloat16)
    queries = queries.reshape(seqs_here, kv_count, group_size, head_size)
    new_key = (
        jnp.dot(normed, w_key, preferred_element_type=jnp.float32)
        .astype(jnp.bfloat16)
        .reshape(seqs_here, kv_count, head_size)
    )
    new_value = (
        jnp.dot(normed, w_value, preferred_element_type=jnp.float32)
        .astype(jnp.bfloat16)
        .reshape(seqs_here, kv_count, head_size)
    )
    log_forget = jax.nn.log_sigmoid(
        jnp.dot(normed, w_forget, preferred_element_type=jnp.float32) + forget_bias
    )
    heads_out = attend(
        queries, new_key, new_value, log_forget, cache_keys, cache_values, cache_gates, lengths
    )
    partial_attn = jnp.dot(heads_out, w_out, preferred_element_type=jnp.float32)
    lanes = lax.broadcasted_iota(jnp.int32, (1, 1, EXTRA), 2)
    route_weight = group_weights[:, None] * expert_weights
    route = jnp.sum(
        jnp.where(expert_ids[:, :, None] == lanes, route_weight[:, :, None], 0.0), axis=1
    ).astype(jnp.bfloat16)
    first = lax.reduce_precision(dense_gate_vector, 8, 7)
    second = lax.reduce_precision(dense_gate_vector - first, 8, 7)
    third = dense_gate_vector - first - second
    vector = jnp.stack([first, second, third], axis=1).astype(jnp.bfloat16)
    wd = jnp.concatenate(
        [
            dense_gate_w,
            jnp.zeros((model_width, 64), jnp.bfloat16),
            dense_up_w,
            vector,
            jnp.zeros((model_width, 61), jnp.bfloat16),
        ],
        axis=1,
    )
    return run_layer(
        partial_attn.astype(jnp.bfloat16),
        inputs,
        norm_gain_ffn.reshape(1, -1),
        route,
        exp_gate[0],
        exp_up[0],
        wd,
        exp_down[0],
        dense_down_w,
    )


def solution(mesh):
    torus = Mesh(mesh.devices.reshape(8, 4, 4, mesh.shape["tp"]), ("ep_0", "ep_1", "ep_2", "tp"))
    placed = (
        P(EP, None),
        P(),
        P(None, "tp"),
        P(None, "tp"),
        P(None, "tp"),
        P(None, "tp"),
        P("tp"),
        P(EP, "tp", None, None),
        P(EP, "tp", None, None),
        P(EP, "tp", None),
        P(EP),
        P("tp", None),
        P(),
        P(EP, None),
        P(EP),
        P(EP, None),
        P(EP, None, "tp"),
        P(EP, None, "tp"),
        P(EP, "tp", None),
        P(),
        P(None, EP_TP),
        P(None, EP_TP),
        P(EP_TP, None),
    )
    return jax.shard_map(
        shards, mesh=torus, in_specs=placed, out_specs=P(EP, "tp"), check_vma=False
    )
```

time: 553 us -> 118 us (0.21)
  waiting for transfers between devices: 439 us -> 0 us
  Pallas kernels: 0 us -> 92.2 us
  blocking collectives: 44.9 us -> 0 us
  matrix products: 27.1 us -> 4.79 us
  starting transfers between devices: 17.4 us -> 0 us
  between operations: 13.7 us -> 0.19 us
  local copies, waits for them, and re-layouts: 5.43 us -> 14.9 us
    reduce_scatter x1 -> x0, waiting for transfers between devices: 319 us -> none  [shards(): lax.psum_scatter(jnp.dot(activated, dense_down_w, preferred_element_type=...]
    pallas_call x0 -> x1, Pallas kernels: none -> 92.2 us  [run_layer(): pl.pallas_call(layer_kernel, out_shape=jax.ShapeDtypeStruct((ROWS, HALF),...]
    all_gather x1 -> x0, waiting for transfers between devices: 80.3 us -> none  [gather_axes(): nearer = lax.all_gather(value, axes[-1], axis=dim, tiled=True)]
    all_to_all x2 -> x0, waiting for transfers between devices: 39.7 us -> none  [the longest x1 23.4 us: shards(): lax.all_to_all(outgoing, EP, split_axis=0, concat_axis=0, tiled=True)]
    all_to_all x3 -> x0, blocking collectives: 24 us -> none  [the longest x1 9.73 us: shards(): lax.all_to_all(shares.astype(jnp.bfloat16), 'tp', split_axis=1, concat_ax...]
    dot_general x7 -> x0, matrix products: 21.3 us -> none  [the longest x1 10.2 us: shards(): jnp.dot(activated, dense_down_w, preferred_element_type=jnp.float32)]
    all_gather x2 -> x0, blocking collectives: 20.9 us -> none  [gather_axes(): nearer = lax.all_gather(value, axes[-1], axis=dim, tiled=True)]
    all_to_all x2 -> x0, starting transfers between devices: 17.3 us -> none  [the longest x1 11.1 us: shards(): lax.all_to_all(outgoing, EP, split_axis=0, concat_axis=0, tiled=True)]
  transfers between devices with their start and end apart: 4 -> 0, of which waited for: 4 -> 0; matrix products, arithmetic and copies ran while one was open for 2% -> 0% of each run, Pallas kernels for 0% -> 0%
where the time goes in v1:
time: 118 us; the launch traced here: 116 us
  Pallas kernels  92.2 us (78%)
  local copies, waits for them, and re-layouts  14.9 us (13%)
  matrix products  4.79 us (4%)
  other arithmetic  4.11 us (3%)
    pallas_call x1, Pallas kernels, run_layer(): pl.pallas_call(layer_kernel, out_shape=jax.ShapeDtypeStruct((ROWS, HALF),...  92.2 us
    unnamed x35, local copies, waits for them, and re-layouts  5.67 us
    concatenate x1, local copies, waits for them, and re-layouts, shards(): jnp.concatenate([dense_gate_w, jnp.zeros((model_width, 64), jnp.bfloat16)...  4.15 us
    another operation x3, local copies, waits for them, and re-layouts, shards(): vector = jnp.stack([first, second, third], axis=1).astype(jnp.bfloat16)  3.12 us

profile of v1, /device:TPU:1, one launch (start us, length us, event | category | flops | bytes accessed | tf_op | source)
XLA Modules:
  0.0 116.1 jit_solution(6660371348552853269)
XLA Ops:
  0.0 0.0 copy-start
  0.0 0.0 copy-start.5
  0.0 1.1 fusion.25
  1.1 1.6 %convolution_convert_fusion.1 = bf16[16,384]{1,0:T(8,128)(2,1)S(1)} fusion(bf16[1536,384]{1,0:T(8,128)(2,1)} %param.25, bf16[16,1536]{1,0:T(8,128)(2,1)} %inp_ref.1, f32[1536]{0:T(1024)} %param.24, f32[16]{0:T(128)S(1)} %add_rsqrt_fusion), kind=kOutput, calls=%fused_computation.10 | convolution fusion | flops 18978816 | bytes 1247296 | tf_op jit(solution)/shard_map/dot_general | solution.py:493
  2.7 0.0 copy-start.3
  2.7 0.0 copy-start.7
  2.7 0.0 copy-start.14
  2.7 0.1 reshape.127
  2.8 0.7 broadcast_add_fusion
  3.5 0.1 iota_compare_fusion
  3.6 1.1 select_reduce_fusion
  4.7 1.0 fusion.33
  5.8 0.1 copy.39
  5.8 0.0 copy-start.15
  5.9 0.8 iota_compare_fusion.1
  6.6 0.0 copy-done
  6.6 0.0 copy-done.5
  6.7 0.0 copy-start.13
  6.7 0.6 fusion.39
  7.3 0.0 copy-done.3
  7.3 0.0 copy-done.7
  7.3 0.0 copy-done.14
  7.3 0.2 fusion.20
  7.5 0.2 fusion.29
  7.6 0.0 copy-start.6
  7.7 0.2 fusion.22
  7.9 0.0 copy-done.15
  7.9 0.2 fusion.19
  8.1 0.2 copy-done.13
  8.3 0.0 copy-start.9
  8.3 0.7 fusion.16
  9.0 0.1 convert_element_type.54
  9.1 0.0 copy-done.6
  9.1 0.3 convolution_convert_fusion.pa_ref
  9.4 0.0 copy-done.9
  9.4 1.1 stack.17
  10.5 1.0 stack.18
  11.5 1.0 stack.19
  12.5 1.9 %copy.41 = bf16[1536,64]{1,0:T(8,128)(2,1)} copy(bf16[1536,64]{0,1:T(8,128)(2,1)} %param.43) | data formatting | bytes 393216 | tf_op args[20]
  14.4 1.8 %copy.42 = bf16[1536,64]{1,0:T(8,128)(2,1)} copy(bf16[1536,64]{0,1:T(8,128)(2,1)} %param.44) | data formatting | bytes 393216 | tf_op args[21]
  16.2 0.0 copy-start.11
  16.2 0.0 copy-start.12
  16.2 0.0 copy-start.10
  16.2 0.0 copy-start.8
  16.2 0.0 copy-start.1
  16.3 0.0 copy-start.4
  16.3 0.8 broadcast_in_dim.61
  17.1 0.8 broadcast_in_dim.62
  17.9 4.1 %concatenate.4.wd_ref = bf16[1536,256]{1,0:T(8,128)(2,1)} concatenate(bf16[1536,64]{1,0:T(8,128)(2,1)} %copy.41, bf16[1536,64]{1,0:T(8,128)(2,1)} %broadcast_in_dim.61, bf16[1536,64]{1,0:T(8,128)(2,1)} %copy.42, bf16[1536,1]{1,0:T(8,128)(2,1)} %stack.17, bf16[1536,1]{1,0:T(8,128)(2,1)} %stack.18, bf16[1536,1]{1,0:T(8,128)(2,1)} %stack.19, bf16[1536,61]{1,0:T(8,128)(2,1)} %broadcast_in_dim.62), dimensions={1} | concatenate | bytes 1572864 | tf_op jit(solution)/shard_map/concatenate | solution.py:521
  22.0 0.0 copy-done.11
  22.0 0.0 copy-done.12
  22.1 0.0 copy-done.10
  22.1 0.1 select_reduce_fusion.1.route_ref
  22.2 0.0 copy-done.8
  22.2 0.0 copy-done.1
  22.2 0.0 copy-done.4
  22.2 0.0 copy-start.2
  22.2 1.1 copy-done.2
  23.3 92.2 %layer.1 = bf16[16,768]{1,0:T(8,128)(2,1)S(1)} custom-call(bf16[16,1536]{1,0:T(8,128)(2,1)S(1)} %convolution_convert_fusion.pa_ref, bf16[16,1536]{1,0:T(8,128)(2,1)S(1)} %copy-done.3, f32[1,1536]{1,0:T(1,128)S(1)} %reshape.130.gain_ref, bf16[16,128]{1,0:T(8,128)(2,1)S(1)} %select_reduce_fusion.1.route_ref, bf16[1536,256]{1,0:T(8,128)(2,1)S(1)} %bitcast.33, ...), custom_call_target="tpu_custom_call" | custom-call | tf_op jit(solution)/shard_map/layer/pallas_call | solution.py:390
  115.5 0.6 copy.54
  (6 shorter events, 0.1 us)
Async XLA Ops:
  0.0 6.6 %copy-start = (bf16[16,1,1024,64]{2,3,1,0:T(8,128)(2,1)S(1)}, bf16[16,1,1024,64]{2,3,1,0:T(8,128)(2,1)}, u32[]{:S(2)}) copy-start(bf16[16,1,1024,64]{2,3,1,0:T(8,128)(2,1)} %param.30) | copy-start | bytes 6291460
  0.0 6.6 %copy-start.5 = (f32[16,6,1024]{2,0,1:T(8,128)S(1)}, f32[16,6,1024]{2,0,1:T(8,128)}, u32[]{:S(2)}) copy-start(f32[16,6,1024]{2,0,1:T(8,128)} %param.32) | copy-start | bytes 1179652
  2.7 4.5 %copy-start.3 = (bf16[16,1536]{1,0:T(8,128)(2,1)S(1)}, bf16[16,1536]{1,0:T(8,128)(2,1)}, u32[]{:S(2)}) copy-start(bf16[16,1536]{1,0:T(8,128)(2,1)} %inp_ref.1) | copy-start | bytes 147460
  2.7 4.5 %copy-start.7 = (f32[1536]{0:T(1024)S(1)}, f32[1536]{0:T(1024)}, u32[]{:S(2)}) copy-start(f32[1536]{0:T(1024)} %param.24) | copy-start | bytes 18436
  2.7 4.5 %copy-start.14 = (bf16[1536,64]{0,1:T(8,128)(2,1)S(1)}, bf16[1536,64]{0,1:T(8,128)(2,1)}, u32[]{:S(2)}) copy-start(bf16[1536,64]{0,1:T(8,128)(2,1)} %param.26) | copy-start | bytes 589828
  5.8 2.1 %copy-start.15 = (bf16[1536,64]{0,1:T(8,128)(2,1)S(1)}, bf16[1536,64]{0,1:T(8,128)(2,1)}, u32[]{:S(2)}) copy-start(bf16[1536,64]{0,1:T(8,128)(2,1)} %param.27) | copy-start | bytes 589828
  6.7 1.6 %copy-start.13 = (bf16[16,1,1024,64]{2,3,1,0:T(8,128)(2,1)S(1)}, bf16[16,1,1024,64]{2,3,1,0:T(8,128)(2,1)}, u32[]{:S(2)}) copy-start(bf16[16,1,1024,64]{2,3,1,0:T(8,128)(2,1)} %param.31) | copy-start | bytes 6291460
  7.6 1.5 %copy-start.6 = (bf16[384,1536]{1,0:T(8,128)(2,1)S(1)}, bf16[384,1536]{1,0:T(8,128)(2,1)}, u32[]{:S(2)}) copy-start(bf16[384,1536]{1,0:T(8,128)(2,1)} %param.34) | copy-start | bytes 3538948
  8.3 1.1 copy-start.9
  16.2 5.8 %copy-start.11 = (f32[16,6]{0,1:T(8,128)S(1)}, f32[16,6]{0,1:T(8,128)}, u32[]{:S(2)}) copy-start(f32[16,6]{0,1:T(8,128)} %param.38) | copy-start | bytes 1156
  16.2 5.8 %copy-start.12 = (f32[16]{0:T(128)S(1)}, f32[16]{0:T(128)}, u32[]{:S(2)}) copy-start(f32[16]{0:T(128)} %param.37) | copy-start | bytes 196
  16.2 5.8 %copy-start.10 = (s32[16,6]{0,1:T(8,128)S(1)}, s32[16,6]{0,1:T(8,128)}, u32[]{:S(2)}) copy-start(s32[16,6]{0,1:T(8,128)} %param.36) | copy-start | bytes 1156
  16.2 5.9 %copy-start.8 = (f32[1536]{0:T(1024)S(1)}, f32[1536]{0:T(1024)}, u32[]{:S(2)}) copy-start(f32[1536]{0:T(1024)} %param.35) | copy-start | bytes 18436
  16.2 5.9 %copy-start.1 = (bf16[1,1536,256]{2,1,0:T(8,128)(2,1)S(1)}, bf16[1,1536,256]{2,1,0:T(8,128)(2,1)}, u32[]{:S(2)}) copy-start(bf16[1,1536,256]{2,1,0:T(8,128)(2,1)} %param.39) | copy-start | bytes 2359300
  16.3 5.9 %copy-start.4 = (bf16[64,1536]{1,0:T(8,128)(2,1)S(1)}, bf16[64,1536]{1,0:T(8,128)(2,1)}, u32[]{:S(2)}) copy-start(bf16[64,1536]{1,0:T(8,128)(2,1)} %dd_ref.1) | copy-start | bytes 589828
  22.2 1.1 copy-start.2

commit v2 on v1

--- a/solution.py
+++ b/solution.py
@@ -25,11 +25,13 @@
 K_AU = 9
 K_AV = 15
 K_PUSH = 21
-K_PART = 25
-K_RV = 29
-K_RU = 35
-K_ZR = 41
-N_SEM = 49
+K_PART = 28
+K_RV = 35
+K_RU = 45
+K_ZR = 51
+N_SEM = 59
+
+PIECES = ((-1, 0), (1, 1), (-1, 1), (1, 0), (2, 0), (2, 1))
 
 
 def mod4(value):
@@ -47,10 +49,14 @@
     route_ref,
     wg_ref,
     wu_ref,
-    wd_ref,
+    dg_ref,
+    du_ref,
+    vec_ref,
     ed_ref,
     dd_ref,
     out_ref,
+    wd,
+    down,
     pr,
     aa,
     xs,
@@ -135,6 +141,21 @@
         for dz in (4, 3, 5, 2, 6, 1, 7):
             send(block, block, K_ZG + dz, (lax.rem(z + dz, 8), y, x, t), K_ZG + zz_own)
 
+    vector = vec_ref[...]
+    first = vector.astype(jnp.bfloat16).astype(jnp.float32)
+    second = (vector - first).astype(jnp.bfloat16).astype(jnp.float32)
+    third = vector - first - second
+    line = lax.broadcasted_iota(jnp.int32, (ROWS, WIDTH), 0)
+    stacked = jnp.where(line == 0, first, jnp.where(line == 1, second, third))
+    wd[0:64] = dg_ref[...]
+    wd[64:128] = jnp.zeros((64, WIDTH), jnp.bfloat16)
+    wd[128:192] = du_ref[...]
+    wd[192:208] = jnp.where(line < 3, stacked, 0.0).astype(jnp.bfloat16)
+    wd[208:256] = jnp.zeros((48, WIDTH), jnp.bfloat16)
+    down[0:256] = ed_ref[...]
+    down[256:320] = dd_ref[...]
+    down[320:384] = jnp.zeros((64, WIDTH), jnp.bfloat16)
+
     for zz in range(4):
 
         @pl.when(4 * t + zz != z)
@@ -170,128 +191,150 @@
 
     ring_gather(piece_v, v, v_plus, v_minus, K_AV)
 
-    def push(w, slot):
-        sent.append(send(xs.at[0, w], xs.at[1, w], K_PUSH + slot, partner))
-
-    push(v, 0)
-
+    f32 = jnp.float32
+    bf16 = jnp.bfloat16
     lane = lax.broadcasted_iota(jnp.int32, (1, EXTRA), 1)
 
-    def unit(side, w):
-        rows = xs[side, w].reshape(16 * ROWS, ROW)
+    def unit(side, one, two):
+        (w_one, half_one), (w_two, half_two) = one, two
+        rows = jnp.concatenate(
+            [
+                xs[side, w_one, 2 * half_one : 2 * half_one + 2].reshape(8 * ROWS, ROW),
+                xs[side, w_two, 2 * half_two : 2 * half_two + 2].reshape(8 * ROWS, ROW),
+            ],
+            axis=0,
+        )
         tokens = rows[:, :WIDTH]
         weight = jnp.sum(
-            jnp.where(lane == expert, rows[:, WIDTH:].astype(jnp.float32), 0.0),
-            axis=1,
-            keepdims=True,
+            jnp.where(lane == expert, rows[:, WIDTH:].astype(f32), 0.0), axis=1, keepdims=True
         )
-        gate = jnp.dot(tokens, wg_ref[...], preferred_element_type=jnp.float32)
-        up = jnp.dot(tokens, wu_ref[...], preferred_element_type=jnp.float32)
-        hidden = (silu(gate) * up * weight).astype(jnp.bfloat16)
-        both = jnp.dot(tokens, wd_ref[...], preferred_element_type=jnp.float32)
-        second = both[:, EXTRA:]
+        gate = jnp.dot(tokens, wg_ref[...], preferred_element_type=f32)
+        up = jnp.dot(tokens, wu_ref[...], preferred_element_type=f32)
+        hidden = (silu(gate) * up * weight).astype(bf16)
+        both = lax.dot_general(
+            tokens, wd[...], (((1,), (1,)), ((), ())), preferred_element_type=f32
+        )
+        second_half = both[:, EXTRA:]
         logit = jnp.sum(
-            jnp.where((lane >= 64) & (lane < 67), second, 0.0), axis=1, keepdims=True
+            jnp.where((lane >= 64) & (lane < 67), second_half, 0.0), axis=1, keepdims=True
         )
         gating = 1.0 / (1.0 + jnp.exp(-logit))
-        dense = (silu(both[:, :EXTRA]) * second * gating).astype(jnp.bfloat16)
-        total = jnp.dot(hidden, ed_ref[...], preferred_element_type=jnp.float32)
-        total = total + jnp.dot(dense[:, :64], dd_ref[...], preferred_element_type=jnp.float32)
-        po[side, w] = total.astype(jnp.bfloat16).reshape(4, 4, ROWS, WIDTH)
-
-    def give(w, slot):
-        sent.append(send(po.at[1, w], dr.at[w], K_PART + slot, partner))
-
-    def received(w, slot):
-        landed(xs.at[1, w], K_PUSH + slot)
-
-    unit(0, v)
-    received(u, 0)
-    unit(1, u)
-    give(u, 0)
-
-    ring_relay(piece_v, v, v_plus, v_minus, K_AV)
-    landed(piece_v(1, mod4(v - 1)), K_AV + 1)
-    push(mod4(v - 1), 1)
-    landed(piece_v(0, mod4(v + 1)), K_AV + 3)
-    push(mod4(v + 1), 2)
-    received(mod4(u - 1), 1)
-    received(mod4(u + 1), 2)
-
-    def middle(i, carry):
-        side = i // 2
-        w = mod4((1 - side) * v + side * u + 2 * lax.rem(i, 2) - 1)
-        unit(side, w)
-        return carry
-
-    lax.fori_loop(0, 4, middle, 0)
-    give(mod4(u - 1), 1)
-    give(mod4(u + 1), 2)
-
-    landed(piece_v(0, mod4(v + 2)), K_AV + 4)
-    landed(piece_v(1, mod4(v + 2)), K_AV + 5)
-    push(mod4(v + 2), 3)
-    received(mod4(u + 2), 3)
-
-    def last(i, carry):
-        side = 1 - i
-        unit(side, mod4((1 - side) * v + side * u + 2))
-        return carry
-
-    lax.fori_loop(0, 2, last, 0)
-    give(mod4(u + 2), 3)
-
-    f32 = jnp.float32
-    bf16 = jnp.bfloat16
-
-    def add_partner(w, slot):
-        landed(dr.at[w], K_PART + slot)
-
+        dense = (silu(both[:, :EXTRA]) * second_half * gating).astype(bf16)
+        hidden = jnp.concatenate([hidden, dense], axis=1)
+        total = jnp.dot(hidden, down[...], preferred_element_type=f32).astype(bf16)
+        total = total.reshape(2, 2, 4, ROWS, WIDTH)
+        po[side, w_one, 2 * half_one : 2 * half_one + 2] = total[0]
+        po[side, w_two, 2 * half_two : 2 * half_two + 2] = total[1]
+
+    def half_of(half):
+        return pl.ds(2 * half, 2)
+
+    def piece_at(base, j):
+        step, half = PIECES[j]
+        return mod4(base + step), half
+
+    def push(j):
+        w, half = piece_at(v, j)
+        piece = xs.at[0, w, half_of(half)]
+        sent.append(send(piece, xs.at[1, w, half_of(half)], K_PUSH + 1 + j, partner))
+
+    def received(j):
+        w, half = piece_at(u, j)
+        landed(xs.at[1, w, half_of(half)], K_PUSH + 1 + j)
+
+    def give(j):
+        w, half = piece_at(u, j)
+        sent.append(
+            send(po.at[1, w, half_of(half)], dr.at[w, half_of(half)], K_PART + 1 + j, partner)
+        )
+
+    def add_into(target, source, count):
         def body(i, carry):
             zz, uu = i // 4, lax.rem(i, 4)
-            both = po[0, w, zz, uu].astype(f32) + dr[w, zz, uu].astype(f32)
-            po[0, w, zz, uu] = both.astype(bf16)
+            target[zz, uu] = (target[zz, uu].astype(f32) + source[zz, uu].astype(f32)).astype(bf16)
             return carry
 
-        lax.fori_loop(0, 16, body, 0)
+        lax.fori_loop(0, 4 * count, body, 0)
+
+    def take(j):
+        w, half = piece_at(v, j)
+        landed(dr.at[w, half_of(half)], K_PART + 1 + j)
+        add_into(po.at[0, w, half_of(half)], dr.at[w, half_of(half)], 2)
 
     right, left, far = mod4(v + 1), mod4(v - 1), mod4(v + 2)
-    low, high = pl.ds(0, 2), pl.ds(2, 2)
-    add_partner(far, 3)
-    sent.append(send(po.at[0, far, low], va, K_RV, v_plus))
-    sent.append(send(po.at[0, far, high], vb, K_RV + 1, v_minus))
-    add_partner(right, 2)
-    sent.append(send(po.at[0, right, high], vf.at[1], K_RV + 2, v_plus))
-    add_partner(left, 1)
-    sent.append(send(po.at[0, left, low], vf.at[0], K_RV + 3, v_minus))
-    add_partner(v, 0)
-
-    landed(va, K_RV)
-
-    def add_a(i, carry):
-        zz, uu = i // 4, lax.rem(i, 4)
-        po[0, right, zz, uu] = (
-            po[0, right, zz, uu].astype(f32) + va[zz, uu].astype(f32)
-        ).astype(bf16)
-        return carry
-
-    lax.fori_loop(0, 8, add_a, 0)
-    sent.append(send(po.at[0, right, low], vf.at[2], K_RV + 4, v_plus))
-    landed(vb, K_RV + 1)
-
-    def add_b(i, carry):
-        zz, uu = i // 4, lax.rem(i, 4)
-        po[0, left, 2 + zz, uu] = (
-            po[0, left, 2 + zz, uu].astype(f32) + vb[zz, uu].astype(f32)
-        ).astype(bf16)
-        return carry
-
-    lax.fori_loop(0, 8, add_b, 0)
-    sent.append(send(po.at[0, left, high], vf.at[3], K_RV + 5, v_minus))
-    landed(vf.at[0], K_RV + 3)
-    landed(vf.at[1], K_RV + 2)
-    landed(vf.at[2], K_RV + 4)
-    landed(vf.at[3], K_RV + 5)
+
+    sent.append(send(xs.at[0, v], xs.at[1, v], K_PUSH, partner))
+    unit(0, (v, 0), (v, 1))
+    landed(xs.at[1, u], K_PUSH)
+    unit(1, (u, 0), (u, 1))
+    sent.append(send(po.at[1, u], dr.at[u], K_PART, partner))
+
+    ring_relay(piece_v, v, v_plus, v_minus, K_AV)
+    push(0)
+    push(1)
+    unit(0, piece_at(v, 0), piece_at(v, 1))
+    received(0)
+    received(1)
+    unit(1, piece_at(u, 0), piece_at(u, 1))
+    give(0)
+    give(1)
+
+    landed(piece_v(1, left), K_AV + 1)
+    push(2)
+    landed(piece_v(0, right), K_AV + 3)
+    push(3)
+    unit(0, piece_at(v, 2), piece_at(v, 3))
+    take(0)
+    sent.append(send(po.at[0, left, half_of(0)], vf.at[0], K_RV + 1, v_minus))
+    take(1)
+    sent.append(send(po.at[0, right, half_of(1)], vf.at[1], K_RV, v_plus))
+    received(2)
+    received(3)
+    unit(1, piece_at(u, 2), piece_at(u, 3))
+    give(2)
+    give(3)
+
+    landed(piece_v(0, far), K_AV + 4)
+    push(4)
+    landed(piece_v(1, far), K_AV + 5)
+    push(5)
+    unit(0, piece_at(v, 4), piece_at(v, 5))
+    received(4)
+    received(5)
+    unit(1, piece_at(u, 4), piece_at(u, 5))
+    give(4)
+    give(5)
+    take(2)
+    take(3)
+
+    take(4)
+    for i in range(2):
+        sent.append(send(po.at[0, far, i], va.at[i], K_RV + 2 + i, v_plus))
+    take(5)
+    for i in range(2):
+        sent.append(send(po.at[0, far, 2 + i], vb.at[i], K_RV + 4 + i, v_minus))
+    landed(dr.at[v], K_PART)
+    add_into(po.at[0, v], dr.at[v], 4)
+
+    def add_row(target, source):
+        def body(uu, carry):
+            target[uu] = (target[uu].astype(f32) + source[uu].astype(f32)).astype(bf16)
+            return carry
+
+        lax.fori_loop(0, 4, body, 0)
+
+    for i in range(2):
+        landed(va.at[i], K_RV + 2 + i)
+        add_row(po.at[0, right, i], va.at[i])
+        sent.append(send(po.at[0, right, i], vf.at[2, i], K_RV + 6 + i, v_plus))
+        landed(vb.at[i], K_RV + 4 + i)
+        add_row(po.at[0, left, 2 + i], vb.at[i])
+        sent.append(send(po.at[0, left, 2 + i], vf.at[3, i], K_RV + 8 + i, v_minus))
+    landed(vf.at[0], K_RV + 1)
+    landed(vf.at[1], K_RV)
+    for i in range(2):
+        landed(vf.at[2, i], K_RV + 6 + i)
+        landed(vf.at[3, i], K_RV + 8 + i)
 
     def add_v(i, carry):
         zz, uu = i // 4, lax.rem(i, 4)
@@ -305,6 +348,7 @@
         return carry
 
     lax.fori_loop(0, 16, add_v, 0)
+    low, high = half_of(0), half_of(1)
 
     right, left, far = mod4(u + 1), mod4(u - 1), mod4(u + 2)
     sent.append(send(sv.at[far, low], ua, K_RU, u_plus))
@@ -384,15 +428,17 @@
                 sent_out(su.at[zz, h], K_ZR + zz * 2 + h)
 
 
-def run_layer(pa, inputs, gain, route, wg, wu, wd, ed, dd):
+def run_layer(pa, inputs, gain, route, wg, wu, dg, du, vector, ed, dd):
     bf16 = jnp.bfloat16
     vmem = pl.BlockSpec(memory_space=pltpu.VMEM)
     return pl.pallas_call(
         layer_kernel,
         out_shape=jax.ShapeDtypeStruct((ROWS, HALF), bf16),
-        in_specs=[vmem] * 9,
+        in_specs=[vmem] * 11,
         out_specs=vmem,
         scratch_shapes=[
+            pltpu.VMEM((256, WIDTH), bf16),
+            pltpu.VMEM((384, WIDTH), bf16),
             pltpu.VMEM((ROWS, WIDTH), bf16),
             pltpu.VMEM((ROWS, WIDTH), jnp.float32),
             pltpu.VMEM((2, 4, 4, 4, ROWS, ROW), bf16),
@@ -414,7 +460,7 @@
             collective_id=0, has_side_effects=True, vmem_limit_bytes=52 * 1024 * 1024
         ),
         name="layer",
-    )(pa, inputs, gain, route, wg, wu, wd, ed, dd)
+    )(pa, inputs, gain, route, wg, wu, dg, du, vector, ed, dd)
 
 
 def rms_scale(row_block, gain):
@@ -514,20 +560,6 @@
     route = jnp.sum(
         jnp.where(expert_ids[:, :, None] == lanes, route_weight[:, :, None], 0.0), axis=1
     ).astype(jnp.bfloat16)
-    first = lax.reduce_precision(dense_gate_vector, 8, 7)
-    second = lax.reduce_precision(dense_gate_vector - first, 8, 7)
-    third = dense_gate_vector - first - second
-    vector = jnp.stack([first, second, third], axis=1).astype(jnp.bfloat16)
-    wd = jnp.concatenate(
-        [
-            dense_gate_w,
-            jnp.zeros((model_width, 64), jnp.bfloat16),
-            dense_up_w,
-            vector,
-            jnp.zeros((model_width, 61), jnp.bfloat16),
-        ],
-        axis=1,
-    )
     return run_layer(
         partial_attn.astype(jnp.bfloat16),
         inputs,
@@ -535,7 +567,9 @@
         route,
         exp_gate[0],
         exp_up[0],
-        wd,
+        dense_gate_w.T,
+        dense_up_w.T,
+        dense_gate_vector.reshape(1, -1),
         exp_down[0],
         dense_down_w,
     )

time: 118 us -> 93.9 us (0.80); the launches traced: 116 us -> 93.5 us
  local copies, waits for them, and re-layouts: 14.9 us -> 1.87 us
  Pallas kernels: 92.2 us -> 80 us
  matrix products: 4.79 us -> 6.68 us
    pallas_call x1, Pallas kernels: 92.2 us -> 80 us  [run_layer(): pl.pallas_call(layer_kernel, out_shape=jax.ShapeDtypeStruct((ROWS, HALF),...]
    unnamed x35 -> x29, local copies, waits for them, and re-layouts: 5.67 us -> 0.82 us
    concatenate x1 -> x0, local copies, waits for them, and re-layouts: 4.15 us -> none  [shards(): jnp.concatenate([dense_gate_w, jnp.zeros((model_width, 64), jnp.bfloat16)...]
    another operation x4 -> x1, local copies, waits for them, and re-layouts: 3.22 us -> 0.09 us  [the longest x3 3.12 us: shards(): vector = jnp.stack([first, second, third], axis=1).astype(jnp.bfloat16)]
    broadcast_in_dim x2 -> x0, local copies, waits for them, and re-layouts: 1.62 us -> none  [the longest x1 0.82 us: shards(): jnp.zeros((model_width, 64), jnp.bfloat16)]
    dot_general x1, matrix products: 0.26 us -> 1.53 us  [shards(): partial_attn = jnp.dot(heads_out, w_out, preferred_element_type=jnp.float32)]
where the time goes in v2:
time: 93.9 us; the launch traced here: 93.5 us
  Pallas kernels  80 us (85%)
  matrix products  6.68 us (7%)
  other arithmetic  4.79 us (5%)
  local copies, waits for them, and re-layouts  1.87 us (2%)
    pallas_call x1, Pallas kernels, run_layer(): pl.pallas_call(layer_kernel, out_shape=jax.ShapeDtypeStruct((ROWS, HALF),...  80 us

profile of v2, /device:TPU:1, one launch (start us, length us, event | category | flops | bytes accessed | tf_op | source)
XLA Modules:
  0.0 93.5 jit_solution(9173575882233983329)
XLA Ops:
  0.0 0.0 copy-start
  0.0 0.0 copy-start.6
  0.0 1.1 %fusion.25 = f32[16]{0:T(128)S(1)} fusion(bf16[16,1536]{1,0:T(8,128)(2,1)} %inp_ref.1), kind=kLoop, calls=%fused_computation.26 | loop fusion | flops 73712 | bytes 49216 | tf_op jit(solution)/shard_map/reduce_sum | solution.py:468
  1.1 1.6 %convolution_convert_fusion.1 = bf16[16,384]{1,0:T(8,128)(2,1)S(1)} fusion(bf16[1536,384]{1,0:T(8,128)(2,1)} %param.25, bf16[16,1536]{1,0:T(8,128)(2,1)} %inp_ref.1, f32[1536]{0:T(1024)} %param.24, f32[16]{0:T(128)S(1)} %add_rsqrt_fusion), kind=kOutput, calls=%fused_computation.10 | convolution fusion | flops 18978816 | bytes 1247296 | tf_op jit(solution)/shard_map/dot_general | solution.py:539
  2.7 0.0 copy-start.2
  2.7 0.0 copy-start.7
  2.7 0.0 copy-start.12
  2.7 0.1 reshape.130
  2.8 0.7 broadcast_add_fusion
  3.5 0.1 iota_compare_fusion
  3.6 1.1 %select_reduce_fusion = f32[16,6]{0,1:T(8,128)S(1)} fusion(f32[16,6,1024]{2,0,1:T(8,128)} %param.32, pred[16,1024]{1,0:T(8,128)(4,1)S(1)} %iota_compare_fusion), kind=kLoop, calls=%fused_computation.21 | loop fusion | flops 196512 | bytes 409984 | tf_op jit(solution)/shard_map/reduce_sum | solution.py:475
  4.7 1.0 %fusion.32 = f32[16,6]{0,1:T(8,128)S(1)} fusion(f32[16,6]{0,1:T(8,128)S(1)} %select_reduce_fusion, bf16[1536,6]{0,1:T(8,128)(2,1)} %param.28, f32[6]{0:T(128)} %param.29, bf16[16,1536]{1,0:T(8,128)(2,1)} %inp_ref.1, f32[1536]{0:T(1024)} %param.24, f32[16]{0:T(128)S(1)} %add_rsqrt_fusion), kind=kOutput, calls=%fused_computation.41 | convolution fusion | flops 394176 | bytes 74584 | tf_op jit(solution)/shard_map/dot_general | solution.py:552
  5.8 0.0 copy-start.13
  5.8 0.1 copy.32
  5.9 0.8 iota_compare_fusion.1
  6.6 0.0 copy-done
  6.6 0.0 copy-done.6
  6.6 0.0 copy-start.11
  6.7 0.6 fusion.38
  7.3 0.0 copy-done.2
  7.3 0.0 copy-done.7
  7.3 0.0 copy-done.12
  7.3 0.2 fusion.20
  7.5 0.1 fusion.28
  7.6 0.3 fusion.22
  7.9 0.0 copy-done.13
  7.9 0.2 fusion.19
  8.1 0.1 copy-done.11
  8.3 0.0 copy-start.10
  8.3 0.0 copy-start.8
  8.3 0.0 copy-start.9
  8.3 0.0 copy-start.1
  8.3 0.0 copy-start.3
  8.3 0.0 copy-start.4
  8.3 0.0 copy-start.5
  8.3 1.3 %fusion.16 = bf16[16,6,64]{2,1,0:T(8,128)(2,1)} fusion(bf16[16,1,1024,64]{2,3,1,0:T(8,128)(2,1)S(1)} %copy-done.11, f32[16,6,1024]{2,1,0:T(8,128)S(1)} %get-tuple-element.8, f32[16,6]{1,0:T(8,128)S(1)} %get-tuple-element.6, f32[16,6]{1,0:T(8,128)S(1)} %multiply_maximum_fusion, f32[16,64]{1,0:T(8,128)S(1)} %fusion.19, f32[16,6]{1,0:T(8,128)S(1)} %get-tuple-element.5), kind=kOutput, calls=%fused_computation.9 | convolution fusion | flops 12896256 | bytes 2507904 | tf_op jit(solution)/shard_map/skgl,skld->skgd/dot_general | solution.py:498
  9.6 0.9 convert_element_type.53
  10.5 1.5 %convolution_convert_fusion.pa_ref = bf16[16,1536]{1,0:T(8,128)(2,1)S(1)} fusion(bf16[16,384]{1,0:T(8,128)(2,1)S(1)} %convert_element_type.53, bf16[384,1536]{1,0:T(8,128)(2,1)} %param.34), kind=kOutput, calls=%fused_computation | convolution fusion | flops 18898944 | bytes 1241088 | tf_op jit(solution)/shard_map/dot_general | solution.py:557
  12.0 0.7 broadcast_multiply_fusion
  12.7 0.0 copy-done.10
  12.7 0.1 select_reduce_fusion.1.route_ref
  12.8 0.0 copy-done.8
  12.8 0.0 copy-done.9
  12.9 0.0 copy-done.1
  12.9 0.0 copy-done.3
  12.9 0.0 copy-done.4
  12.9 0.0 copy-done.5
  12.9 80.0 %layer.1 = bf16[16,768]{1,0:T(8,128)(2,1)S(1)} custom-call(bf16[16,1536]{1,0:T(8,128)(2,1)S(1)} %convolution_convert_fusion.pa_ref, bf16[16,1536]{1,0:T(8,128)(2,1)S(1)} %copy-done.2, f32[1,1536]{1,0:T(1,128)S(1)} %reshape.133.gain_ref, bf16[16,128]{1,0:T(8,128)(2,1)S(1)} %select_reduce_fusion.1.route_ref, bf16[1536,256]{1,0:T(8,128)(2,1)S(1)} %bitcast.35, ...), custom_call_target="tpu_custom_call" | custom-call | tf_op jit(solution)/shard_map/layer/pallas_call | solution.py:434
  92.9 0.6 copy.42
  (5 shorter events, 0.0 us)
Async XLA Ops:
  0.0 6.6 %copy-start = (bf16[16,1,1024,64]{2,3,1,0:T(8,128)(2,1)S(1)}, bf16[16,1,1024,64]{2,3,1,0:T(8,128)(2,1)}, u32[]{:S(2)}) copy-start(bf16[16,1,1024,64]{2,3,1,0:T(8,128)(2,1)} %param.30) | copy-start | bytes 6291460
  0.0 6.6 %copy-start.6 = (f32[16,6,1024]{2,0,1:T(8,128)S(1)}, f32[16,6,1024]{2,0,1:T(8,128)}, u32[]{:S(2)}) copy-start(f32[16,6,1024]{2,0,1:T(8,128)} %param.32) | copy-start | bytes 1179652
  2.7 4.5 %copy-start.2 = (bf16[16,1536]{1,0:T(8,128)(2,1)S(1)}, bf16[16,1536]{1,0:T(8,128)(2,1)}, u32[]{:S(2)}) copy-start(bf16[16,1536]{1,0:T(8,128)(2,1)} %inp_ref.1) | copy-start | bytes 147460
  2.7 4.5 %copy-start.7 = (f32[1536]{0:T(1024)S(1)}, f32[1536]{0:T(1024)}, u32[]{:S(2)}) copy-start(f32[1536]{0:T(1024)} %param.24) | copy-start | bytes 18436
  2.7 4.5 %copy-start.12 = (bf16[1536,64]{0,1:T(8,128)(2,1)S(1)}, bf16[1536,64]{0,1:T(8,128)(2,1)}, u32[]{:S(2)}) copy-start(bf16[1536,64]{0,1:T(8,128)(2,1)} %param.26) | copy-start | bytes 589828
  5.8 2.1 %copy-start.13 = (bf16[1536,64]{0,1:T(8,128)(2,1)S(1)}, bf16[1536,64]{0,1:T(8,128)(2,1)}, u32[]{:S(2)}) copy-start(bf16[1536,64]{0,1:T(8,128)(2,1)} %param.27) | copy-start | bytes 589828
  6.6 1.6 %copy-start.11 = (bf16[16,1,1024,64]{2,3,1,0:T(8,128)(2,1)S(1)}, bf16[16,1,1024,64]{2,3,1,0:T(8,128)(2,1)}, u32[]{:S(2)}) copy-start(bf16[16,1,1024,64]{2,3,1,0:T(8,128)(2,1)} %param.31) | copy-start | bytes 6291460
  8.3 4.5 %copy-start.10 = (s32[16,6]{0,1:T(8,128)S(1)}, s32[16,6]{0,1:T(8,128)}, u32[]{:S(2)}) copy-start(s32[16,6]{0,1:T(8,128)} %param.36) | copy-start | bytes 1156
  8.3 4.6 %copy-start.8 = (f32[1536]{0:T(1024)S(1)}, f32[1536]{0:T(1024)}, u32[]{:S(2)}) copy-start(f32[1536]{0:T(1024)} %param.35) | copy-start | bytes 18436
  8.3 4.6 %copy-start.9 = (f32[1536]{0:T(1024)S(1)}, f32[1536]{0:T(1024)}, u32[]{:S(2)}) copy-start(f32[1536]{0:T(1024)} %param.42) | copy-start | bytes 18436
  8.3 4.6 %copy-start.1 = (bf16[1,1536,256]{2,1,0:T(8,128)(2,1)S(1)}, bf16[1,1536,256]{2,1,0:T(8,128)(2,1)}, u32[]{:S(2)}) copy-start(bf16[1,1536,256]{2,1,0:T(8,128)(2,1)} %param.39) | copy-start | bytes 2359300
  8.3 4.6 %copy-start.3 = (bf16[1536,64]{0,1:T(8,128)(2,1)S(1)}, bf16[1536,64]{0,1:T(8,128)(2,1)}, u32[]{:S(2)}) copy-start(bf16[1536,64]{0,1:T(8,128)(2,1)} %param.43) | copy-start | bytes 589828
  8.3 4.6 %copy-start.4 = (bf16[1536,64]{0,1:T(8,128)(2,1)S(1)}, bf16[1536,64]{0,1:T(8,128)(2,1)}, u32[]{:S(2)}) copy-start(bf16[1536,64]{0,1:T(8,128)(2,1)} %param.44) | copy-start | bytes 589828
  8.3 4.6 %copy-start.5 = (bf16[64,1536]{1,0:T(8,128)(2,1)S(1)}, bf16[64,1536]{1,0:T(8,128)(2,1)}, u32[]{:S(2)}) copy-start(bf16[64,1536]{1,0:T(8,128)(2,1)} %dd_ref.1) | copy-start | bytes 589828

commit v3 on v2

--- a/solution.py
+++ b/solution.py
@@ -23,15 +23,15 @@
 K_PA = 0
 K_ZG = 1
 K_AU = 9
-K_AV = 15
-K_PUSH = 21
-K_PART = 28
-K_RV = 35
-K_RU = 45
-K_ZR = 51
-N_SEM = 59
-
-PIECES = ((-1, 0), (1, 1), (-1, 1), (1, 0), (2, 0), (2, 1))
+K_ZR = 15
+K_RU = 23
+K_AV = 29
+K_PUSH = 53
+K_PART = 69
+K_RV = 73
+N_SEM = 97
+
+STAGES = (0, 1, 2, -1)
 
 
 def mod4(value):
@@ -162,48 +162,60 @@
         def _():
             landed(xs.at[0, v, zz, u], K_ZG + zz)
 
-    def ring_gather(piece, w, plus, minus, k):
-        own_a, own_b = piece(0, w), piece(1, w)
+    f32 = jnp.float32
+    bf16 = jnp.bfloat16
+    right, left, far = mod4(v + 1), mod4(v - 1), mod4(v + 2)
+    low, high = pl.ds(0, 2), pl.ds(2, 2)
+
+    def ring_send(piece, w, plus, minus, k):
+        own_a, own_b = piece(low, w), piece(high, w)
         sent.append(send(own_a, own_a, k, plus))
         sent.append(send(own_b, own_b, k + 2, minus))
         sent.append(send(own_b, own_b, k + 1, plus))
         sent.append(send(own_a, own_a, k + 3, minus))
 
     def ring_relay(piece, w, plus, minus, k):
-        a_left, b_right = piece(0, mod4(w - 1)), piece(1, mod4(w + 1))
+        a_left, b_right = piece(low, mod4(w - 1)), piece(high, mod4(w + 1))
         landed(a_left, k)
         sent.append(send(a_left, a_left, k + 4, plus))
         landed(b_right, k + 2)
         sent.append(send(b_right, b_right, k + 5, minus))
 
     def piece_u(half, w):
-        return xs.at[0, v, pl.ds(2 * half, 2), w]
-
-    def piece_v(half, w):
-        return xs.at[0, w, pl.ds(2 * half, 2)]
-
-    ring_gather(piece_u, u, u_plus, u_minus, K_AU)
-    ring_relay(piece_u, u, u_plus, u_minus, K_AU)
-    landed(piece_u(1, mod4(u - 1)), K_AU + 1)
-    landed(piece_u(0, mod4(u + 1)), K_AU + 3)
-    landed(piece_u(0, mod4(u + 2)), K_AU + 4)
-    landed(piece_u(1, mod4(u + 2)), K_AU + 5)
-
-    ring_gather(piece_v, v, v_plus, v_minus, K_AV)
-
-    f32 = jnp.float32
-    bf16 = jnp.bfloat16
+        return xs.at[0, v, half, w]
+
+    def column(n):
+        return mod4(u + STAGES[n])
+
+    def piece_v(n):
+        return lambda half, w: xs.at[0, w, half, column(n)]
+
+    def push(n, w, slot):
+        piece = xs.at[0, w, :, column(n)]
+        sent.append(send(piece, xs.at[1, w, :, column(n)], K_PUSH + 4 * n + slot, partner))
+
+    def gather_send(n):
+        ring_send(piece_v(n), v, v_plus, v_minus, K_AV + 6 * n)
+        push(n, v, 0)
+
+    def gather_relay(n):
+        ring_relay(piece_v(n), v, v_plus, v_minus, K_AV + 6 * n)
+
+    def gather_near(n):
+        landed(piece_v(n)(high, left), K_AV + 6 * n + 1)
+        push(n, left, 1)
+        landed(piece_v(n)(low, right), K_AV + 6 * n + 3)
+        push(n, right, 2)
+
+    def gather_far(n):
+        landed(piece_v(n)(low, far), K_AV + 6 * n + 4)
+        landed(piece_v(n)(high, far), K_AV + 6 * n + 5)
+        push(n, far, 3)
+
     lane = lax.broadcasted_iota(jnp.int32, (1, EXTRA), 1)
 
-    def unit(side, one, two):
-        (w_one, half_one), (w_two, half_two) = one, two
-        rows = jnp.concatenate(
-            [
-                xs[side, w_one, 2 * half_one : 2 * half_one + 2].reshape(8 * ROWS, ROW),
-                xs[side, w_two, 2 * half_two : 2 * half_two + 2].reshape(8 * ROWS, ROW),
-            ],
-            axis=0,
-        )
+    def unit(side, col):
+        rows = xs[side, :, :, col].reshape(16 * ROWS, ROW)
         tokens = rows[:, :WIDTH]
         weight = jnp.sum(
             jnp.where(lane == expert, rows[:, WIDTH:].astype(f32), 0.0), axis=1, keepdims=True
@@ -222,151 +234,123 @@
         dense = (silu(both[:, :EXTRA]) * second_half * gating).astype(bf16)
         hidden = jnp.concatenate([hidden, dense], axis=1)
         total = jnp.dot(hidden, down[...], preferred_element_type=f32).astype(bf16)
-        total = total.reshape(2, 2, 4, ROWS, WIDTH)
-        po[side, w_one, 2 * half_one : 2 * half_one + 2] = total[0]
-        po[side, w_two, 2 * half_two : 2 * half_two + 2] = total[1]
-
-    def half_of(half):
-        return pl.ds(2 * half, 2)
-
-    def piece_at(base, j):
-        step, half = PIECES[j]
-        return mod4(base + step), half
-
-    def push(j):
-        w, half = piece_at(v, j)
-        piece = xs.at[0, w, half_of(half)]
-        sent.append(send(piece, xs.at[1, w, half_of(half)], K_PUSH + 1 + j, partner))
-
-    def received(j):
-        w, half = piece_at(u, j)
-        landed(xs.at[1, w, half_of(half)], K_PUSH + 1 + j)
-
-    def give(j):
-        w, half = piece_at(u, j)
-        sent.append(
-            send(po.at[1, w, half_of(half)], dr.at[w, half_of(half)], K_PART + 1 + j, partner)
-        )
+        po[side, :, :, col] = total.reshape(4, 4, ROWS, WIDTH)
+
+    def own_unit(n):
+        unit(0, column(n))
+
+    def partner_unit(n):
+        col = mod4(v + STAGES[n])
+        for slot, step in enumerate((0, -1, 1, 2)):
+            landed(xs.at[1, mod4(u + step), :, col], K_PUSH + 4 * n + slot)
+        unit(1, col)
+        sent.append(send(po.at[1, :, :, col], dr.at[:, :, col], K_PART + n, partner))
 
     def add_into(target, source, count):
-        def body(i, carry):
-            zz, uu = i // 4, lax.rem(i, 4)
-            target[zz, uu] = (target[zz, uu].astype(f32) + source[zz, uu].astype(f32)).astype(bf16)
-            return carry
-
-        lax.fori_loop(0, 4 * count, body, 0)
-
-    def take(j):
-        w, half = piece_at(v, j)
-        landed(dr.at[w, half_of(half)], K_PART + 1 + j)
-        add_into(po.at[0, w, half_of(half)], dr.at[w, half_of(half)], 2)
-
-    right, left, far = mod4(v + 1), mod4(v - 1), mod4(v + 2)
-
-    sent.append(send(xs.at[0, v], xs.at[1, v], K_PUSH, partner))
-    unit(0, (v, 0), (v, 1))
-    landed(xs.at[1, u], K_PUSH)
-    unit(1, (u, 0), (u, 1))
-    sent.append(send(po.at[1, u], dr.at[u], K_PART, partner))
-
-    ring_relay(piece_v, v, v_plus, v_minus, K_AV)
-    push(0)
-    push(1)
-    unit(0, piece_at(v, 0), piece_at(v, 1))
-    received(0)
-    received(1)
-    unit(1, piece_at(u, 0), piece_at(u, 1))
-    give(0)
-    give(1)
-
-    landed(piece_v(1, left), K_AV + 1)
-    push(2)
-    landed(piece_v(0, right), K_AV + 3)
-    push(3)
-    unit(0, piece_at(v, 2), piece_at(v, 3))
-    take(0)
-    sent.append(send(po.at[0, left, half_of(0)], vf.at[0], K_RV + 1, v_minus))
-    take(1)
-    sent.append(send(po.at[0, right, half_of(1)], vf.at[1], K_RV, v_plus))
-    received(2)
-    received(3)
-    unit(1, piece_at(u, 2), piece_at(u, 3))
-    give(2)
-    give(3)
-
-    landed(piece_v(0, far), K_AV + 4)
-    push(4)
-    landed(piece_v(1, far), K_AV + 5)
-    push(5)
-    unit(0, piece_at(v, 4), piece_at(v, 5))
-    received(4)
-    received(5)
-    unit(1, piece_at(u, 4), piece_at(u, 5))
-    give(4)
-    give(5)
-    take(2)
-    take(3)
-
-    take(4)
-    for i in range(2):
-        sent.append(send(po.at[0, far, i], va.at[i], K_RV + 2 + i, v_plus))
-    take(5)
-    for i in range(2):
-        sent.append(send(po.at[0, far, 2 + i], vb.at[i], K_RV + 4 + i, v_minus))
-    landed(dr.at[v], K_PART)
-    add_into(po.at[0, v], dr.at[v], 4)
-
-    def add_row(target, source):
-        def body(uu, carry):
-            target[uu] = (target[uu].astype(f32) + source[uu].astype(f32)).astype(bf16)
-            return carry
-
-        lax.fori_loop(0, 4, body, 0)
-
-    for i in range(2):
-        landed(va.at[i], K_RV + 2 + i)
-        add_row(po.at[0, right, i], va.at[i])
-        sent.append(send(po.at[0, right, i], vf.at[2, i], K_RV + 6 + i, v_plus))
-        landed(vb.at[i], K_RV + 4 + i)
-        add_row(po.at[0, left, 2 + i], vb.at[i])
-        sent.append(send(po.at[0, left, 2 + i], vf.at[3, i], K_RV + 8 + i, v_minus))
-    landed(vf.at[0], K_RV + 1)
-    landed(vf.at[1], K_RV)
-    for i in range(2):
-        landed(vf.at[2, i], K_RV + 6 + i)
-        landed(vf.at[3, i], K_RV + 8 + i)
-
-    def add_v(i, carry):
-        zz, uu = i // 4, lax.rem(i, 4)
-        half, inner = zz // 2, lax.rem(zz, 2)
-        total = (
-            po[0, v, zz, uu].astype(f32)
-            + vf[half, inner, uu].astype(f32)
-            + vf[2 + half, inner, uu].astype(f32)
-        )
-        sv[uu, zz] = total.astype(bf16)
-        return carry
-
-    lax.fori_loop(0, 16, add_v, 0)
-    low, high = half_of(0), half_of(1)
-
-    right, left, far = mod4(u + 1), mod4(u - 1), mod4(u + 2)
-    sent.append(send(sv.at[far, low], ua, K_RU, u_plus))
-    sent.append(send(sv.at[far, high], ub, K_RU + 1, u_minus))
-    sent.append(send(sv.at[right, high], uf.at[1], K_RU + 2, u_plus))
-    sent.append(send(sv.at[left, low], uf.at[0], K_RU + 3, u_minus))
+        for i in range(count):
+            target[i] = (target[i].astype(f32) + source[i].astype(f32)).astype(bf16)
+
+    def reduce_send(n):
+        col = column(n)
+        k = K_RV + 6 * n
+        landed(dr.at[:, :, col], K_PART + n)
+
+        def take(w):
+            add_into(po.at[0, w, :, col], dr.at[w, :, col], 4)
+
+        take(far)
+        sent.append(send(po.at[0, far, low, col], va.at[col], k, v_plus))
+        sent.append(send(po.at[0, far, high, col], vb.at[col], k + 1, v_minus))
+        take(right)
+        sent.append(send(po.at[0, right, high, col], vf.at[1, col], k + 2, v_plus))
+        take(left)
+        sent.append(send(po.at[0, left, low, col], vf.at[0, col], k + 3, v_minus))
+
+    def reduce_relay(n):
+        col = column(n)
+        k = K_RV + 6 * n
+        landed(va.at[col], k)
+        add_into(po.at[0, right, low, col], va.at[col], 2)
+        sent.append(send(po.at[0, right, low, col], vf.at[2, col], k + 4, v_plus))
+        landed(vb.at[col], k + 1)
+        add_into(po.at[0, left, high, col], vb.at[col], 2)
+        sent.append(send(po.at[0, left, high, col], vf.at[3, col], k + 5, v_minus))
+
+    def reduce_end(n):
+        col = column(n)
+        k = K_RV + 6 * n
+        landed(vf.at[0, col], k + 3)
+        landed(vf.at[1, col], k + 2)
+        landed(vf.at[2, col], k + 4)
+        landed(vf.at[3, col], k + 5)
+        for zz in range(4):
+            half, inner = zz // 2, zz % 2
+            total = (
+                po[0, v, zz, col].astype(f32)
+                + dr[v, zz, col].astype(f32)
+                + vf[half, col, inner].astype(f32)
+                + vf[2 + half, col, inner].astype(f32)
+            )
+            sv[col, zz] = total.astype(bf16)
+
+    ring_send(piece_u, u, u_plus, u_minus, K_AU)
+    gather_send(0)
+    ring_relay(piece_u, u, u_plus, u_minus, K_AU)
+    gather_relay(0)
+    landed(piece_u(low, mod4(u + 1)), K_AU + 3)
+    landed(piece_u(high, mod4(u - 1)), K_AU + 1)
+    gather_send(1)
+    landed(piece_u(low, mod4(u + 2)), K_AU + 4)
+    landed(piece_u(high, mod4(u + 2)), K_AU + 5)
+    gather_send(2)
+    gather_near(0)
+    gather_far(0)
+    own_unit(0)
+    gather_relay(1)
+    gather_send(3)
+    partner_unit(0)
+    gather_near(1)
+    gather_relay(2)
+    reduce_send(0)
+    gather_far(1)
+    own_unit(1)
+    gather_near(2)
+    gather_relay(3)
+    partner_unit(1)
+    gather_far(2)
+    own_unit(2)
+    reduce_relay(0)
+    reduce_send(1)
+    gather_near(3)
+    partner_unit(2)
+    gather_far(3)
+    own_unit(3)
+    reduce_relay(1)
+    reduce_send(2)
+    partner_unit(3)
+    reduce_end(0)
+    reduce_end(1)
+
+    up_col, far_col, down_col = column(1), column(2), column(3)
+    sent.append(send(sv.at[up_col, high], uf.at[1], K_RU + 2, u_plus))
+    reduce_relay(2)
+    reduce_send(3)
+    reduce_end(2)
+    sent.append(send(sv.at[far_col, low], ua, K_RU, u_plus))
+    sent.append(send(sv.at[far_col, high], ub, K_RU + 1, u_minus))
+    reduce_relay(3)
     landed(ua, K_RU)
-    for zz in range(2):
-        sv[right, zz] = (sv[right, zz].astype(f32) + ua[zz].astype(f32)).astype(bf16)
-    sent.append(send(sv.at[right, low], uf.at[2], K_RU + 4, u_plus))
+    add_into(sv.at[up_col, low], ua, 2)
+    sent.append(send(sv.at[up_col, low], uf.at[2], K_RU + 4, u_plus))
+    reduce_end(3)
+    sent.append(send(sv.at[down_col, low], uf.at[0], K_RU + 3, u_minus))
     landed(ub, K_RU + 1)
-    for zz in range(2):
-        sv[left, 2 + zz] = (sv[left, 2 + zz].astype(f32) + ub[zz].astype(f32)).astype(bf16)
-    sent.append(send(sv.at[left, high], uf.at[3], K_RU + 5, u_minus))
-    landed(uf.at[0], K_RU + 3)
+    add_into(sv.at[down_col, high], ub, 2)
+    sent.append(send(sv.at[down_col, high], uf.at[3], K_RU + 5, u_minus))
     landed(uf.at[1], K_RU + 2)
     landed(uf.at[2], K_RU + 4)
     landed(uf.at[3], K_RU + 5)
+    landed(uf.at[0], K_RU + 3)
     for zz in range(4):
         half, inner = zz // 2, zz % 2
         total = (
@@ -444,9 +428,9 @@
             pltpu.VMEM((2, 4, 4, 4, ROWS, ROW), bf16),
             pltpu.VMEM((2, 4, 4, 4, ROWS, WIDTH), bf16),
             pltpu.VMEM((4, 4, 4, ROWS, WIDTH), bf16),
-            pltpu.VMEM((2, 4, ROWS, WIDTH), bf16),
-            pltpu.VMEM((2, 4, ROWS, WIDTH), bf16),
-            pltpu.VMEM((4, 2, 4, ROWS, WIDTH), bf16),
+            pltpu.VMEM((4, 2, ROWS, WIDTH), bf16),
+            pltpu.VMEM((4, 2, ROWS, WIDTH), bf16),
+            pltpu.VMEM((4, 4, 2, ROWS, WIDTH), bf16),
             pltpu.VMEM((4, 4, ROWS, WIDTH), bf16),
             pltpu.VMEM((2, ROWS, WIDTH), bf16),
             pltpu.VMEM((2, ROWS, WIDTH), bf16),

time: 93.9 us -> 88 us (0.937)
  Pallas kernels: 80 us -> 74.1 us
    pallas_call x1, Pallas kernels: 80 us -> 74.1 us  [run_layer(): pl.pallas_call(layer_kernel, out_shape=jax.ShapeDtypeStruct((ROWS, HALF),...]
where the time goes in v3:
time: 88 us; the launch traced here: 87.6 us
  Pallas kernels  74.1 us (84%)
  matrix products  6.68 us (8%)
  other arithmetic  4.79 us (5%)
  local copies, waits for them, and re-layouts  1.87 us (2%)
    pallas_call x1, Pallas kernels, run_layer(): pl.pallas_call(layer_kernel, out_shape=jax.ShapeDtypeStruct((ROWS, HALF),...  74.1 us

profile of v3, /device:TPU:1, one launch (start us, length us, event | category | flops | bytes accessed | tf_op | source)
XLA Modules:
  0.0 87.6 jit_solution(4014072337361239172)
XLA Ops:
  0.0 0.0 copy-start
  0.0 0.0 copy-start.6
  0.0 1.1 %fusion.25 = f32[16]{0:T(128)S(1)} fusion(bf16[16,1536]{1,0:T(8,128)(2,1)} %inp_ref.1), kind=kLoop, calls=%fused_computation.26 | loop fusion | flops 73712 | bytes 49216 | tf_op jit(solution)/shard_map/reduce_sum | solution.py:452
  1.1 1.6 %convolution_convert_fusion.1 = bf16[16,384]{1,0:T(8,128)(2,1)S(1)} fusion(bf16[1536,384]{1,0:T(8,128)(2,1)} %param.25, bf16[16,1536]{1,0:T(8,128)(2,1)} %inp_ref.1, f32[1536]{0:T(1024)} %param.24, f32[16]{0:T(128)S(1)} %add_rsqrt_fusion), kind=kOutput, calls=%fused_computation.10 | convolution fusion | flops 18978816 | bytes 1247296 | tf_op jit(solution)/shard_map/dot_general | solution.py:523
  2.7 0.0 copy-start.2
  2.7 0.0 copy-start.7
  2.7 0.0 copy-start.12
  2.7 0.1 reshape.130
  2.8 0.7 broadcast_add_fusion
  3.5 0.1 iota_compare_fusion
  3.6 1.1 %select_reduce_fusion = f32[16,6]{0,1:T(8,128)S(1)} fusion(f32[16,6,1024]{2,0,1:T(8,128)} %param.32, pred[16,1024]{1,0:T(8,128)(4,1)S(1)} %iota_compare_fusion), kind=kLoop, calls=%fused_computation.21 | loop fusion | flops 196512 | bytes 409984 | tf_op jit(solution)/shard_map/reduce_sum | solution.py:459
  4.7 1.0 %fusion.32 = f32[16,6]{0,1:T(8,128)S(1)} fusion(f32[16,6]{0,1:T(8,128)S(1)} %select_reduce_fusion, bf16[1536,6]{0,1:T(8,128)(2,1)} %param.28, f32[6]{0:T(128)} %param.29, bf16[16,1536]{1,0:T(8,128)(2,1)} %inp_ref.1, f32[1536]{0:T(1024)} %param.24, f32[16]{0:T(128)S(1)} %add_rsqrt_fusion), kind=kOutput, calls=%fused_computation.41 | convolution fusion | flops 394176 | bytes 74584 | tf_op jit(solution)/shard_map/dot_general | solution.py:536
  5.8 0.0 copy-start.13
  5.8 0.1 copy.32
  5.9 0.8 iota_compare_fusion.1
  6.6 0.0 copy-done
  6.6 0.0 copy-done.6
  6.6 0.0 copy-start.11
  6.7 0.6 fusion.38
  7.3 0.0 copy-done.2
  7.3 0.0 copy-done.7
  7.3 0.0 copy-done.12
  7.3 0.2 fusion.20
  7.5 0.1 fusion.28
  7.6 0.3 fusion.22
  7.9 0.0 copy-done.13
  7.9 0.2 fusion.19
  8.1 0.1 copy-done.11
  8.3 0.0 copy-start.10
  8.3 0.0 copy-start.8
  8.3 0.0 copy-start.9
  8.3 0.0 copy-start.1
  8.3 0.0 copy-start.3
  8.3 0.0 copy-start.4
  8.3 0.0 copy-start.5
  8.3 1.3 %fusion.16 = bf16[16,6,64]{2,1,0:T(8,128)(2,1)} fusion(bf16[16,1,1024,64]{2,3,1,0:T(8,128)(2,1)S(1)} %copy-done.11, f32[16,6,1024]{2,1,0:T(8,128)S(1)} %get-tuple-element.8, f32[16,6]{1,0:T(8,128)S(1)} %get-tuple-element.6, f32[16,6]{1,0:T(8,128)S(1)} %multiply_maximum_fusion, f32[16,64]{1,0:T(8,128)S(1)} %fusion.19, f32[16,6]{1,0:T(8,128)S(1)} %get-tuple-element.5), kind=kOutput, calls=%fused_computation.9 | convolution fusion | flops 12896256 | bytes 2507904 | tf_op jit(solution)/shard_map/skgl,skld->skgd/dot_general | solution.py:482
  9.6 0.9 convert_element_type.53
  10.5 1.5 %convolution_convert_fusion.pa_ref = bf16[16,1536]{1,0:T(8,128)(2,1)S(1)} fusion(bf16[16,384]{1,0:T(8,128)(2,1)S(1)} %convert_element_type.53, bf16[384,1536]{1,0:T(8,128)(2,1)} %param.34), kind=kOutput, calls=%fused_computation | convolution fusion | flops 18898944 | bytes 1241088 | tf_op jit(solution)/shard_map/dot_general | solution.py:541
  12.0 0.7 broadcast_multiply_fusion
  12.7 0.0 copy-done.10
  12.7 0.1 select_reduce_fusion.1.route_ref
  12.8 0.0 copy-done.8
  12.8 0.0 copy-done.9
  12.9 0.0 copy-done.1
  12.9 0.0 copy-done.3
  12.9 0.0 copy-done.4
  12.9 0.0 copy-done.5
  12.9 74.1 %layer.1 = bf16[16,768]{1,0:T(8,128)(2,1)S(1)} custom-call(bf16[16,1536]{1,0:T(8,128)(2,1)S(1)} %convolution_convert_fusion.pa_ref, bf16[16,1536]{1,0:T(8,128)(2,1)S(1)} %copy-done.2, f32[1,1536]{1,0:T(1,128)S(1)} %reshape.133.gain_ref, bf16[16,128]{1,0:T(8,128)(2,1)S(1)} %select_reduce_fusion.1.route_ref, bf16[1536,256]{1,0:T(8,128)(2,1)S(1)} %bitcast.35, ...), custom_call_target="tpu_custom_call" | custom-call | tf_op jit(solution)/shard_map/layer/pallas_call | solution.py:418
  87.0 0.6 copy.42
  (5 shorter events, 0.0 us)
Async XLA Ops:
  0.0 6.6 %copy-start = (bf16[16,1,1024,64]{2,3,1,0:T(8,128)(2,1)S(1)}, bf16[16,1,1024,64]{2,3,1,0:T(8,128)(2,1)}, u32[]{:S(2)}) copy-start(bf16[16,1,1024,64]{2,3,1,0:T(8,128)(2,1)} %param.30) | copy-start | bytes 6291460
  0.0 6.6 %copy-start.6 = (f32[16,6,1024]{2,0,1:T(8,128)S(1)}, f32[16,6,1024]{2,0,1:T(8,128)}, u32[]{:S(2)}) copy-start(f32[16,6,1024]{2,0,1:T(8,128)} %param.32) | copy-start | bytes 1179652
  2.7 4.5 %copy-start.2 = (bf16[16,1536]{1,0:T(8,128)(2,1)S(1)}, bf16[16,1536]{1,0:T(8,128)(2,1)}, u32[]{:S(2)}) copy-start(bf16[16,1536]{1,0:T(8,128)(2,1)} %inp_ref.1) | copy-start | bytes 147460
  2.7 4.5 %copy-start.7 = (f32[1536]{0:T(1024)S(1)}, f32[1536]{0:T(1024)}, u32[]{:S(2)}) copy-start(f32[1536]{0:T(1024)} %param.24) | copy-start | bytes 18436
  2.7 4.5 %copy-start.12 = (bf16[1536,64]{0,1:T(8,128)(2,1)S(1)}, bf16[1536,64]{0,1:T(8,128)(2,1)}, u32[]{:S(2)}) copy-start(bf16[1536,64]{0,1:T(8,128)(2,1)} %param.26) | copy-start | bytes 589828
  5.8 2.1 %copy-start.13 = (bf16[1536,64]{0,1:T(8,128)(2,1)S(1)}, bf16[1536,64]{0,1:T(8,128)(2,1)}, u32[]{:S(2)}) copy-start(bf16[1536,64]{0,1:T(8,128)(2,1)} %param.27) | copy-start | bytes 589828
  6.6 1.6 %copy-start.11 = (bf16[16,1,1024,64]{2,3,1,0:T(8,128)(2,1)S(1)}, bf16[16,1,1024,64]{2,3,1,0:T(8,128)(2,1)}, u32[]{:S(2)}) copy-start(bf16[16,1,1024,64]{2,3,1,0:T(8,128)(2,1)} %param.31) | copy-start | bytes 6291460
  8.3 4.5 %copy-start.10 = (s32[16,6]{0,1:T(8,128)S(1)}, s32[16,6]{0,1:T(8,128)}, u32[]{:S(2)}) copy-start(s32[16,6]{0,1:T(8,128)} %param.36) | copy-start | bytes 1156
  8.3 4.6 %copy-start.8 = (f32[1536]{0:T(1024)S(1)}, f32[1536]{0:T(1024)}, u32[]{:S(2)}) copy-start(f32[1536]{0:T(1024)} %param.35) | copy-start | bytes 18436
  8.3 4.6 %copy-start.9 = (f32[1536]{0:T(1024)S(1)}, f32[1536]{0:T(1024)}, u32[]{:S(2)}) copy-start(f32[1536]{0:T(1024)} %param.42) | copy-start | bytes 18436
  8.3 4.6 %copy-start.1 = (bf16[1,1536,256]{2,1,0:T(8,128)(2,1)S(1)}, bf16[1,1536,256]{2,1,0:T(8,128)(2,1)}, u32[]{:S(2)}) copy-start(bf16[1,1536,256]{2,1,0:T(8,128)(2,1)} %param.39) | copy-start | bytes 2359300
  8.3 4.6 %copy-start.3 = (bf16[1536,64]{0,1:T(8,128)(2,1)S(1)}, bf16[1536,64]{0,1:T(8,128)(2,1)}, u32[]{:S(2)}) copy-start(bf16[1536,64]{0,1:T(8,128)(2,1)} %param.43) | copy-start | bytes 589828
  8.3 4.6 %copy-start.4 = (bf16[1536,64]{0,1:T(8,128)(2,1)S(1)}, bf16[1536,64]{0,1:T(8,128)(2,1)}, u32[]{:S(2)}) copy-start(bf16[1536,64]{0,1:T(8,128)(2,1)} %param.44) | copy-start | bytes 589828
  8.3 4.6 %copy-start.5 = (bf16[64,1536]{1,0:T(8,128)(2,1)S(1)}, bf16[64,1536]{1,0:T(8,128)(2,1)}, u32[]{:S(2)}) copy-start(bf16[64,1536]{1,0:T(8,128)(2,1)} %dd_ref.1) | copy-start | bytes 589828

commit v4 on v3

--- a/solution.py
+++ b/solution.py
@@ -42,19 +42,183 @@
     return value / (1.0 + jnp.exp(-value))
 
 
-def layer_kernel(
-    pa_ref,
+def att_scratch():
+    bf16, f32 = jnp.bfloat16, jnp.float32
+    return [
+        pltpu.VMEM((1536, 384), bf16),
+        pltpu.VMEM((16, 64, 1024), bf16),
+        pltpu.VMEM((16, 64, 1024), bf16),
+        pltpu.VMEM((6, 16, 1024), f32),
+        pltpu.VMEM((384, 1536), bf16),
+        pltpu.VMEM((128, 128), f32),
+        pltpu.VMEM((1024, 128), f32),
+        pltpu.SemaphoreType.DMA((8,)),
+    ]
+
+
+def att_copies(wq_hbm, ck_hbm, cv_hbm, cg_hbm, wo_hbm, wq, ck, cv, cg, wo, sem):
+    half = pl.ds(0, 8), pl.ds(8, 8)
+    pairs = [
+        (wq_hbm, wq),
+        (ck_hbm.at[half[0]], ck.at[half[0]]),
+        (ck_hbm.at[half[1]], ck.at[half[1]]),
+        (cg_hbm, cg),
+        (cv_hbm.at[half[0]], cv.at[half[0]]),
+        (cv_hbm.at[half[1]], cv.at[half[1]]),
+        (wo_hbm, wo),
+    ]
+    return [pltpu.make_async_copy(src, dst, sem.at[i]) for i, (src, dst) in enumerate(pairs)]
+
+
+def start_loads(wq_hbm, ck_hbm, cv_hbm, cg_hbm, wo_hbm, wq, ck, cv, cg, wo, qs, sc, sem):
+    for copy in att_copies(wq_hbm, ck_hbm, cv_hbm, cg_hbm, wo_hbm, wq, ck, cv, cg, wo, sem):
+        copy.start()
+
+
+def attention(
     inp_ref,
     gain_ref,
-    route_ref,
+    wk_ref,
+    wv_ref,
+    wf_ref,
+    fb_ref,
+    len_ref,
+    wq_hbm,
+    ck_hbm,
+    cv_hbm,
+    cg_hbm,
+    wo_hbm,
+    out_ref,
+    wq,
+    ck,
+    cv,
+    cg,
+    wo,
+    qs,
+    sc,
+    sem,
+):
+    f32, bf16 = jnp.float32, jnp.bfloat16
+    loads = att_copies(wq_hbm, ck_hbm, cv_hbm, cg_hbm, wo_hbm, wq, ck, cv, cg, wo, sem)
+    transposed = (((1,), (1,)), ((), ()))
+    row_block = inp_ref[...].astype(f32)
+    factor = lax.rsqrt(jnp.mean(row_block * row_block, axis=-1, keepdims=True) + EPS)
+    normed = (row_block * factor * gain_ref[...].reshape(1, WIDTH)).astype(bf16)
+    new_key = lax.dot_general(normed, wk_ref[...], transposed, preferred_element_type=f32)
+    new_key = new_key.astype(bf16).astype(f32)
+    new_value = lax.dot_general(normed, wv_ref[...], transposed, preferred_element_type=f32)
+    new_value = new_value.astype(bf16).astype(f32)
+    logit = lax.dot_general(normed, wf_ref[...], transposed, preferred_element_type=f32)
+    loads[0].wait()
+    queries = jnp.dot(normed, wq[...], preferred_element_type=f32).astype(bf16).astype(f32)
+    own_scores = []
+    qs[...] = jnp.zeros((128, 128), f32)
+
+    def head_rows(h):
+        return pl.ds(h, 16, stride=8)
+
+    def load_head(h):
+        return jnp.concatenate(
+            [sc[pl.ds(128 * c + h, 16, stride=8), :] for c in range(8)], axis=1
+        )
+
+    for h in range(6):
+        query = queries[:, 128 * (h // 2) : 128 * (h // 2) + 128]
+        if h % 2:
+            query = pltpu.roll(query, 64, 1)
+        own_scores.append(jnp.sum(query[:, :64] * new_key, axis=1, keepdims=True) * 0.125)
+        qs[head_rows(h), :] = query
+    for s in range(16):
+        if s % 8 == 0:
+            loads[1 + s // 8].wait()
+        scores = jnp.dot(
+            qs[8 * s : 8 * s + 8, :64].astype(bf16), ck[s], preferred_element_type=f32
+        )
+        for c in range(8):
+            sc[128 * c + 8 * s : 128 * c + 8 * s + 8, :] = scores[:, 128 * c : 128 * c + 128]
+    loads[3].wait()
+    line = lax.broadcasted_iota(jnp.int32, (16, 1), 0)
+    counts = jnp.zeros((16, 1), jnp.int32)
+    for s in range(16):
+        counts = jnp.where(line == s, len_ref[s], counts)
+    positions = lax.broadcasted_iota(jnp.int32, (16, 1024), 1)
+    valid = positions < counts
+    newest = positions == counts - 1
+    own_weights = []
+    for h in range(6):
+        gates = cg[h]
+        last = jnp.sum(jnp.where(newest, gates, 0.0), axis=1, keepdims=True)
+        forget = logit[:, h : h + 1] + fb_ref[h]
+        forget = jnp.minimum(forget, 0.0) - jnp.log1p(jnp.exp(-jnp.abs(forget)))
+        offsets = (last + forget) - gates
+        cached = load_head(h) * 0.125 + offsets
+        cached = jnp.where(valid, cached, -jnp.inf)
+        own = own_scores[h]
+        peak = jnp.maximum(jnp.max(cached, axis=1, keepdims=True), own)
+        cached = jnp.exp(cached - peak)
+        own = jnp.exp(own - peak)
+        denominator = jnp.sum(cached, axis=1, keepdims=True) + own
+        cached = cached / denominator
+        for c in range(8):
+            sc[pl.ds(128 * c + h, 16, stride=8), :] = cached[:, 128 * c : 128 * c + 128]
+        own_weights.append((own / denominator).astype(bf16).astype(f32))
+    for s in range(16):
+        if s % 8 == 0:
+            loads[4 + s // 8].wait()
+        weights = jnp.concatenate(
+            [sc[128 * c + 8 * s : 128 * c + 8 * s + 8, :] for c in range(8)], axis=1
+        )
+        qs[8 * s : 8 * s + 8, :64] = lax.dot_general(
+            weights.astype(bf16), cv[s], transposed, preferred_element_type=f32
+        )
+    loads[6].wait()
+    total = jnp.zeros((16, 1536), f32)
+    for h in range(6):
+        head = qs[head_rows(h), :][:, :64] + own_weights[h] * new_value
+        total = total + jnp.dot(
+            head.astype(bf16), wo[64 * h : 64 * h + 64, :], preferred_element_type=f32
+        )
+    out_ref[...] = total.astype(bf16)
+
+
+def layer_kernel(
+    inp_ref,
+    gain_attn_ref,
+    wk_ref,
+    wv_ref,
+    wf_ref,
+    fb_ref,
+    len_ref,
+    wq_hbm,
+    ck_hbm,
+    cv_hbm,
+    cg_hbm,
+    wo_hbm,
+    gain_ref,
+    ids_ref,
+    gw_ref,
+    ew_ref,
+    wg_hbm,
+    wu_hbm,
+    ed_hbm,
+    vec_ref,
+    dg_hbm,
+    du_hbm,
+    dd_hbm,
+    out_ref,
     wg_ref,
     wu_ref,
-    dg_ref,
-    du_ref,
-    vec_ref,
-    ed_ref,
-    dd_ref,
-    out_ref,
+    pa_ref,
+    route,
+    wsem,
+    wq,
+    ck,
+    cv,
+    cg,
+    wo,
+    qs,
+    sc,
+    asem,
     wd,
     down,
     pr,
@@ -113,6 +277,24 @@
             device_id_type=MESH,
         ).wait_recv()
 
+    streams = (wq_hbm, ck_hbm, cv_hbm, cg_hbm, wo_hbm, wq, ck, cv, cg, wo)
+    start_loads(*streams, qs, sc, asem)
+    weight_loads = [
+        pltpu.make_async_copy(src, dst, wsem.at[i])
+        for i, (src, dst) in enumerate(
+            (
+                (wg_hbm, wg_ref),
+                (wu_hbm, wu_ref),
+                (ed_hbm, down.at[pl.ds(0, 256)]),
+                (dd_hbm, down.at[pl.ds(256, 64)]),
+                (dg_hbm, wd.at[pl.ds(0, 64)]),
+                (du_hbm, wd.at[pl.ds(128, 64)]),
+            )
+        )
+    ]
+    for copy in weight_loads:
+        copy.start()
+
     barrier = pltpu.get_barrier_semaphore()
     for device in (partner, u_plus, u_minus, v_plus, v_minus):
         pl.semaphore_signal(barrier, inc=1, device_id=device, device_id_type=MESH)
@@ -121,6 +303,38 @@
             pl.semaphore_signal(
                 barrier, inc=1, device_id=(lax.rem(z + dz, 8), y, x, core), device_id_type=MESH
             )
+
+    table_lane = lax.broadcasted_iota(jnp.int32, (1, EXTRA), 1)
+    for s in range(ROWS):
+        row = jnp.zeros((1, EXTRA), jnp.float32)
+        for choice in range(6):
+            row = jnp.where(
+                table_lane == ids_ref[choice, s], gw_ref[s] * ew_ref[choice, s], row
+            )
+        route[s : s + 1, :] = row
+    attention(
+        inp_ref,
+        gain_attn_ref,
+        wk_ref,
+        wv_ref,
+        wf_ref,
+        fb_ref,
+        len_ref,
+        wq_hbm,
+        ck_hbm,
+        cv_hbm,
+        cg_hbm,
+        wo_hbm,
+        pa_ref,
+        wq,
+        ck,
+        cv,
+        cg,
+        wo,
+        qs,
+        sc,
+        asem,
+    )
     pl.semaphore_wait(barrier, 19)
 
     sent = []
@@ -131,30 +345,28 @@
     after = inp_ref[...].astype(jnp.float32) + attn
     aa[...] = after
     factor = lax.rsqrt(jnp.mean(after * after, axis=-1, keepdims=True) + EPS)
-    normed = (after * factor * gain_ref[...]).astype(jnp.bfloat16)
+    normed = (after * factor * gain_ref[...].reshape(1, WIDTH)).astype(jnp.bfloat16)
 
     @pl.when(part == t)
     def _():
         xs[0, v, zz_own, u, :, :WIDTH] = normed
-        xs[0, v, zz_own, u, :, WIDTH:] = route_ref[...]
+        xs[0, v, zz_own, u, :, WIDTH:] = route[...].astype(jnp.bfloat16)
         block = xs.at[0, v, zz_own, u]
         for dz in (4, 3, 5, 2, 6, 1, 7):
             send(block, block, K_ZG + dz, (lax.rem(z + dz, 8), y, x, t), K_ZG + zz_own)
 
-    vector = vec_ref[...]
+    vector = vec_ref[...].reshape(1, WIDTH)
     first = vector.astype(jnp.bfloat16).astype(jnp.float32)
     second = (vector - first).astype(jnp.bfloat16).astype(jnp.float32)
     third = vector - first - second
     line = lax.broadcasted_iota(jnp.int32, (ROWS, WIDTH), 0)
     stacked = jnp.where(line == 0, first, jnp.where(line == 1, second, third))
-    wd[0:64] = dg_ref[...]
     wd[64:128] = jnp.zeros((64, WIDTH), jnp.bfloat16)
-    wd[128:192] = du_ref[...]
     wd[192:208] = jnp.where(line < 3, stacked, 0.0).astype(jnp.bfloat16)
     wd[208:256] = jnp.zeros((48, WIDTH), jnp.bfloat16)
-    down[0:256] = ed_ref[...]
-    down[256:320] = dd_ref[...]
     down[320:384] = jnp.zeros((64, WIDTH), jnp.bfloat16)
+    for copy in weight_loads:
+        copy.wait()
 
     for zz in range(4):
 
@@ -412,15 +624,30 @@
                 sent_out(su.at[zz, h], K_ZR + zz * 2 + h)
 
 
-def run_layer(pa, inputs, gain, route, wg, wu, dg, du, vector, ed, dd):
+def run_layer(*arrays):
     bf16 = jnp.bfloat16
     vmem = pl.BlockSpec(memory_space=pltpu.VMEM)
+    smem = pl.BlockSpec(memory_space=pltpu.SMEM)
+    hbm = pl.BlockSpec(memory_space=pl.ANY)
     return pl.pallas_call(
         layer_kernel,
         out_shape=jax.ShapeDtypeStruct((ROWS, HALF), bf16),
-        in_specs=[vmem] * 11,
+        in_specs=[vmem] * 5
+        + [smem] * 2
+        + [hbm] * 5
+        + [vmem]
+        + [smem] * 3
+        + [hbm] * 3
+        + [vmem]
+        + [hbm] * 3,
         out_specs=vmem,
         scratch_shapes=[
+            pltpu.VMEM((WIDTH, 256), bf16),
+            pltpu.VMEM((WIDTH, 256), bf16),
+            pltpu.VMEM((ROWS, WIDTH), bf16),
+            pltpu.VMEM((ROWS, EXTRA), jnp.float32),
+            pltpu.SemaphoreType.DMA((6,)),
+            *att_scratch(),
             pltpu.VMEM((256, WIDTH), bf16),
             pltpu.VMEM((384, WIDTH), bf16),
             pltpu.VMEM((ROWS, WIDTH), bf16),
@@ -441,52 +668,10 @@
             pltpu.SemaphoreType.DMA((N_SEM,)),
         ],
         compiler_params=pltpu.CompilerParams(
-            collective_id=0, has_side_effects=True, vmem_limit_bytes=52 * 1024 * 1024
+            collective_id=0, has_side_effects=True, vmem_limit_bytes=60 * 1024 * 1024
         ),
         name="layer",
-    )(pa, inputs, gain, route, wg, wu, dg, du, vector, ed, dd)
-
-
-def rms_scale(row_block, gain):
-    row_block = row_block.astype(jnp.float32)
-    factor = lax.rsqrt(jnp.mean(row_block * row_block, axis=-1, keepdims=True) + EPS)
-    return (row_block * factor * gain).astype(jnp.bfloat16)
-
-
-def attend(queries, new_key, new_value, log_forget, keys, values, gates, counts):
-    seqs_here, kv_count, group_size, head_size = queries.shape
-    cache_positions = lax.broadcasted_iota(jnp.int32, (1, 1, gates.shape[2]), 2)
-    last_gate = jnp.sum(
-        jnp.where(cache_positions == (counts - 1)[:, None, None], gates, 0.0), axis=2
-    )
-    offsets = (last_gate + log_forget)[:, :, None] - gates
-    offsets = offsets.reshape(seqs_here, kv_count, group_size, gates.shape[2])
-    scale_factor = head_size ** (-0.5)
-    cached = (
-        jnp.einsum("skgd,skld->skgl", queries, keys, preferred_element_type=jnp.float32)
-        * scale_factor
-        + offsets
-    )
-    valid_mask = cache_positions.reshape(1, 1, 1, -1) < counts[:, None, None, None]
-    cached = jnp.where(valid_mask, cached, -jnp.inf)
-    own_score = (
-        jnp.einsum("skgd,skd->skg", queries, new_key, preferred_element_type=jnp.float32)
-        * scale_factor
-    )
-    peak_score = jnp.maximum(jnp.max(cached, axis=3), own_score)
-    cached_exp = jnp.exp(cached - peak_score[..., None])
-    own_exp = jnp.exp(own_score - peak_score)
-    denominator = jnp.sum(cached_exp, axis=3) + own_exp
-    cached_weight = (cached_exp / denominator[..., None]).astype(jnp.bfloat16)
-    own_weight = (own_exp / denominator).astype(jnp.bfloat16)
-    mixed_values = jnp.einsum(
-        "skgl,skld->skgd", cached_weight, values, preferred_element_type=jnp.float32
-    )
-    mixed_values = (
-        mixed_values
-        + own_weight.astype(jnp.float32)[..., None] * new_value.astype(jnp.float32)[:, :, None, :]
-    )
-    return mixed_values.reshape(seqs_here, kv_count * group_size * head_size).astype(jnp.bfloat16)
+    )(*arrays)
 
 
 def shards(
@@ -514,47 +699,29 @@
     dense_up_w,
     dense_down_w,
 ):
-    seqs_here, model_width = inputs.shape
-    kv_count = cache_keys.shape[1]
-    head_size = cache_keys.shape[3]
-    heads_here = w_forget.shape[1]
-    group_size = heads_here // kv_count
-    normed = rms_scale(inputs, norm_gain_attn)
-    queries = jnp.dot(normed, w_query, preferred_element_type=jnp.float32).astype(jnp.bfloat16)
-    queries = queries.reshape(seqs_here, kv_count, group_size, head_size)
-    new_key = (
-        jnp.dot(normed, w_key, preferred_element_type=jnp.float32)
-        .astype(jnp.bfloat16)
-        .reshape(seqs_here, kv_count, head_size)
-    )
-    new_value = (
-        jnp.dot(normed, w_value, preferred_element_type=jnp.float32)
-        .astype(jnp.bfloat16)
-        .reshape(seqs_here, kv_count, head_size)
-    )
-    log_forget = jax.nn.log_sigmoid(
-        jnp.dot(normed, w_forget, preferred_element_type=jnp.float32) + forget_bias
-    )
-    heads_out = attend(
-        queries, new_key, new_value, log_forget, cache_keys, cache_values, cache_gates, lengths
-    )
-    partial_attn = jnp.dot(heads_out, w_out, preferred_element_type=jnp.float32)
-    lanes = lax.broadcasted_iota(jnp.int32, (1, 1, EXTRA), 2)
-    route_weight = group_weights[:, None] * expert_weights
-    route = jnp.sum(
-        jnp.where(expert_ids[:, :, None] == lanes, route_weight[:, :, None], 0.0), axis=1
-    ).astype(jnp.bfloat16)
     return run_layer(
-        partial_attn.astype(jnp.bfloat16),
         inputs,
-        norm_gain_ffn.reshape(1, -1),
-        route,
+        norm_gain_attn,
+        w_key.T,
+        w_value.T,
+        w_forget.T,
+        forget_bias,
+        lengths,
+        w_query,
+        cache_keys[:, 0].transpose(0, 2, 1),
+        cache_values[:, 0].transpose(0, 2, 1),
+        cache_gates.transpose(1, 0, 2),
+        w_out,
+        norm_gain_ffn,
+        expert_ids.T,
+        group_weights,
+        expert_weights.T,
         exp_gate[0],
         exp_up[0],
+        exp_down[0],
+        dense_gate_vector,
         dense_gate_w.T,
         dense_up_w.T,
-        dense_gate_vector.reshape(1, -1),
-        exp_down[0],
         dense_down_w,
     )
 

time: 88 us -> 78 us (0.89)
  matrix products: 6.68 us -> 0 us
  other arithmetic: 4.79 us -> 0 us
  Pallas kernels: 74.1 us -> 76.5 us
    dot_general x8 -> x0, matrix products: 6.68 us -> none  [the longest x1 1.63 us: shards(): jnp.dot(normed, w_query, preferred_element_type=jnp.float32)]
    reduce_sum x4 -> x0, other arithmetic: 2.52 us -> none  [the longest x1 1.11 us: attend(): jnp.sum(jnp.where(cache_positions == (counts - 1)[:, None, None], gates,...]
    pallas_call x1, Pallas kernels: 74.1 us -> 76.5 us  [run_layer(): pl.pallas_call(layer_kernel, out_shape=jax.ShapeDtypeStruct((ROWS, HALF),...]
where the time goes in v4:
time: 78 us; the launch traced here: 77.8 us
  Pallas kernels  76.5 us (98%)
  local copies, waits for them, and re-layouts  1.35 us (2%)
    pallas_call x1, Pallas kernels, run_layer(): pl.pallas_call(layer_kernel, out_shape=jax.ShapeDtypeStruct((ROWS, HALF),...  76.5 us

profile of v4, /device:TPU:1, one launch (start us, length us, event | category | flops | bytes accessed | tf_op | source)
XLA Modules:
  0.0 77.8 jit_solution(16524313178302343805)
XLA Ops:
  0.0 76.5 %layer.1 = bf16[16,768]{1,0:T(8,128)(2,1)} custom-call(bf16[16,1536]{1,0:T(8,128)(2,1)} %inp_ref.1, f32[1536]{0:T(1024)} %gain_attn_ref.1, bf16[64,1536]{1,0:T(8,128)(2,1)} %bitcast.23, bf16[64,1536]{1,0:T(8,128)(2,1)} %bitcast.24, bf16[6,1536]{1,0:T(8,128)(2,1)} %bitcast.27, f32[6]{0:T(128)} %fb_ref.1, s32[16]{0:T(128)} %len_ref.1, ...), custom_call_target="tpu_custom_call" | custom-call | tf_op jit(solution)/shard_map/layer/pallas_call | solution.py:632
  76.5 1.3 %copy.25 = bf16[16,768]{1,0:T(8,128)(2,1)} copy(bf16[16,768]{1,0:T(8,128)(2,1)} %layer.1) | data formatting | bytes 49152

commit v5 on v4

--- a/solution.py
+++ b/solution.py
@@ -505,87 +505,86 @@
             )
             sv[col, zz] = total.astype(bf16)
 
+    up_col, far_col, down_col = column(1), column(2), column(3)
     ring_send(piece_u, u, u_plus, u_minus, K_AU)
     gather_send(0)
     ring_relay(piece_u, u, u_plus, u_minus, K_AU)
-    gather_relay(0)
     landed(piece_u(low, mod4(u + 1)), K_AU + 3)
     landed(piece_u(high, mod4(u - 1)), K_AU + 1)
     gather_send(1)
+    gather_relay(0)
     landed(piece_u(low, mod4(u + 2)), K_AU + 4)
     landed(piece_u(high, mod4(u + 2)), K_AU + 5)
+    gather_relay(1)
+    gather_near(0)
     gather_send(2)
-    gather_near(0)
+    gather_near(1)
+    gather_send(3)
     gather_far(0)
     own_unit(0)
-    gather_relay(1)
-    gather_send(3)
+    gather_far(1)
     partner_unit(0)
-    gather_near(1)
     gather_relay(2)
-    reduce_send(0)
-    gather_far(1)
     own_unit(1)
     gather_near(2)
     gather_relay(3)
     partner_unit(1)
+    reduce_send(0)
     gather_far(2)
+    gather_near(3)
     own_unit(2)
-    reduce_relay(0)
+    gather_far(3)
+    partner_unit(2)
     reduce_send(1)
-    gather_near(3)
-    partner_unit(2)
-    gather_far(3)
+    partner_unit(3)
+    reduce_send(2)
     own_unit(3)
+    reduce_send(3)
+    reduce_relay(2)
     reduce_relay(1)
-    reduce_send(2)
-    partner_unit(3)
-    reduce_end(0)
-    reduce_end(1)
-
-    up_col, far_col, down_col = column(1), column(2), column(3)
-    sent.append(send(sv.at[up_col, high], uf.at[1], K_RU + 2, u_plus))
-    reduce_relay(2)
-    reduce_send(3)
+    reduce_relay(3)
     reduce_end(2)
     sent.append(send(sv.at[far_col, low], ua, K_RU, u_plus))
     sent.append(send(sv.at[far_col, high], ub, K_RU + 1, u_minus))
-    reduce_relay(3)
+    reduce_relay(0)
+    reduce_end(1)
+    reduce_end(3)
+    sent.append(send(sv.at[down_col, low], uf.at[0], K_RU + 3, u_minus))
+    sent.append(send(sv.at[up_col, high], uf.at[1], K_RU + 2, u_plus))
     landed(ua, K_RU)
     add_into(sv.at[up_col, low], ua, 2)
     sent.append(send(sv.at[up_col, low], uf.at[2], K_RU + 4, u_plus))
-    reduce_end(3)
-    sent.append(send(sv.at[down_col, low], uf.at[0], K_RU + 3, u_minus))
     landed(ub, K_RU + 1)
     add_into(sv.at[down_col, high], ub, 2)
     sent.append(send(sv.at[down_col, high], uf.at[3], K_RU + 5, u_minus))
-    landed(uf.at[1], K_RU + 2)
-    landed(uf.at[2], K_RU + 4)
-    landed(uf.at[3], K_RU + 5)
-    landed(uf.at[0], K_RU + 3)
-    for zz in range(4):
-        half, inner = zz // 2, zz % 2
-        total = (
-            sv[u, zz].astype(f32)
-            + uf[half, inner].astype(f32)
-            + uf[2 + half, inner].astype(f32)
-        ).astype(bf16)
-        for h in range(2):
-            su[zz, h] = total[:, h * HALF : (h + 1) * HALF]
-
-    for zz in range(4):
-        for h in range(2):
-            here = (4 * t + zz == z) & (t == h)
-
-            @pl.when(jnp.logical_not(here))
-            def _():
-                send(
-                    su.at[zz, h], zr.at[z], K_ZR + zz * 2 + h, (4 * t + zz, y, x, h), K_ZR + z
-                )
-
-            @pl.when(here)
-            def _():
-                zr[z] = su[zz, h]
+    reduce_end(0)
+    for half in range(2):
+        landed(uf.at[half], K_RU + 3 - half)
+        landed(uf.at[2 + half], K_RU + 4 + half)
+        for inner in range(2):
+            zz = 2 * half + inner
+            total = (
+                sv[u, zz].astype(f32)
+                + uf[half, inner].astype(f32)
+                + uf[2 + half, inner].astype(f32)
+            ).astype(bf16)
+            for h in range(2):
+                su[zz, h] = total[:, h * HALF : (h + 1) * HALF]
+                here = (4 * t + zz == z) & (t == h)
+
+                @pl.when(jnp.logical_not(here))
+                def _():
+                    send(
+                        su.at[zz, h],
+                        zr.at[z],
+                        K_ZR + zz * 2 + h,
+                        (4 * t + zz, y, x, h),
+                        K_ZR + z,
+                    )
+
+                @pl.when(here)
+                def _():
+                    zr[z] = su[zz, h]
 
     for s in range(8):
 
@@ -628,7 +627,7 @@
     bf16 = jnp.bfloat16
     vmem = pl.BlockSpec(memory_space=pltpu.VMEM)
     smem = pl.BlockSpec(memory_space=pltpu.SMEM)
-    hbm = pl.BlockSpec(memory_space=pl.ANY)
+    hbm = pl.BlockSpec(memory_space=pltpu.HBM)
     return pl.pallas_call(
         layer_kernel,
         out_shape=jax.ShapeDtypeStruct((ROWS, HALF), bf16),

time: 78 us -> 73.5 us (0.942)
  Pallas kernels: 76.5 us -> 71.8 us
    pallas_call x1, Pallas kernels: 76.5 us -> 71.8 us  [run_layer(): pl.pallas_call(layer_kernel, out_shape=jax.ShapeDtypeStruct((ROWS, HALF),...]
where the time goes in v5:
time: 73.5 us; the launch traced here: 73.1 us
  Pallas kernels  71.8 us (98%)
  local copies, waits for them, and re-layouts  1.35 us (2%)
    pallas_call x1, Pallas kernels, run_layer(): pl.pallas_call(layer_kernel, out_shape=jax.ShapeDtypeStruct((ROWS, HALF),...  71.8 us

profile of v5, /device:TPU:1, one launch (start us, length us, event | category | flops | bytes accessed | tf_op | source)
XLA Modules:
  0.0 73.1 jit_solution(1399688649984997133)
XLA Ops:
  0.0 71.8 %layer.1 = bf16[16,768]{1,0:T(8,128)(2,1)} custom-call(bf16[16,1536]{1,0:T(8,128)(2,1)} %inp_ref.1, f32[1536]{0:T(1024)} %gain_attn_ref.1, bf16[64,1536]{1,0:T(8,128)(2,1)} %bitcast.23, bf16[64,1536]{1,0:T(8,128)(2,1)} %bitcast.24, bf16[6,1536]{1,0:T(8,128)(2,1)} %bitcast.27, f32[6]{0:T(128)} %fb_ref.1, s32[16]{0:T(128)} %len_ref.1, ...), custom_call_target="tpu_custom_call" | custom-call | tf_op jit(solution)/shard_map/layer/pallas_call | solution.py:631
  71.8 1.3 %copy.25 = bf16[16,768]{1,0:T(8,128)(2,1)} copy(bf16[16,768]{1,0:T(8,128)(2,1)} %layer.1) | data formatting | bytes 49152

commit v6 on v5

--- a/solution.py
+++ b/solution.py
@@ -511,53 +511,53 @@
     ring_relay(piece_u, u, u_plus, u_minus, K_AU)
     landed(piece_u(low, mod4(u + 1)), K_AU + 3)
     landed(piece_u(high, mod4(u - 1)), K_AU + 1)
-    gather_send(1)
+    gather_send(3)
     gather_relay(0)
+    gather_near(0)
     landed(piece_u(low, mod4(u + 2)), K_AU + 4)
     landed(piece_u(high, mod4(u + 2)), K_AU + 5)
-    gather_relay(1)
-    gather_near(0)
+    gather_relay(3)
+    gather_near(3)
     gather_send(2)
-    gather_near(1)
-    gather_send(3)
+    gather_send(1)
     gather_far(0)
     own_unit(0)
-    gather_far(1)
+    gather_far(3)
     partner_unit(0)
     gather_relay(2)
-    own_unit(1)
+    partner_unit(3)
+    gather_relay(1)
+    own_unit(3)
     gather_near(2)
-    gather_relay(3)
-    partner_unit(1)
     reduce_send(0)
     gather_far(2)
-    gather_near(3)
     own_unit(2)
-    gather_far(3)
+    gather_near(1)
+    reduce_send(3)
+    gather_far(1)
     partner_unit(2)
+    reduce_relay(0)
+    partner_unit(1)
+    reduce_send(2)
+    own_unit(1)
     reduce_send(1)
-    partner_unit(3)
-    reduce_send(2)
-    own_unit(3)
-    reduce_send(3)
     reduce_relay(2)
+    reduce_relay(3)
     reduce_relay(1)
-    reduce_relay(3)
     reduce_end(2)
     sent.append(send(sv.at[far_col, low], ua, K_RU, u_plus))
     sent.append(send(sv.at[far_col, high], ub, K_RU + 1, u_minus))
-    reduce_relay(0)
+    reduce_end(3)
+    reduce_end(0)
     reduce_end(1)
-    reduce_end(3)
+    sent.append(send(sv.at[up_col, high], uf.at[1], K_RU + 2, u_plus))
     sent.append(send(sv.at[down_col, low], uf.at[0], K_RU + 3, u_minus))
-    sent.append(send(sv.at[up_col, high], uf.at[1], K_RU + 2, u_plus))
     landed(ua, K_RU)
     add_into(sv.at[up_col, low], ua, 2)
     sent.append(send(sv.at[up_col, low], uf.at[2], K_RU + 4, u_plus))
     landed(ub, K_RU + 1)
     add_into(sv.at[down_col, high], ub, 2)
     sent.append(send(sv.at[down_col, high], uf.at[3], K_RU + 5, u_minus))
-    reduce_end(0)
     for half in range(2):
         landed(uf.at[half], K_RU + 3 - half)
         landed(uf.at[2 + half], K_RU + 4 + half)

time: 73.5 us -> 72.9 us (level)
  no operation moved by 1% of the time
where the time goes in v6:
time: 72.9 us; the launch traced here: 72.7 us
  Pallas kernels  71.4 us (98%)
  local copies, waits for them, and re-layouts  1.35 us (2%)
    pallas_call x1, Pallas kernels, run_layer(): pl.pallas_call(layer_kernel, out_shape=jax.ShapeDtypeStruct((ROWS, HALF),...  71.4 us

profile of v6, /device:TPU:1, one launch (start us, length us, event | category | flops | bytes accessed | tf_op | source)
XLA Modules:
  0.0 72.7 jit_solution(5247782104978201523)
XLA Ops:
  0.0 71.4 %layer.1 = bf16[16,768]{1,0:T(8,128)(2,1)} custom-call(bf16[16,1536]{1,0:T(8,128)(2,1)} %inp_ref.1, f32[1536]{0:T(1024)} %gain_attn_ref.1, bf16[64,1536]{1,0:T(8,128)(2,1)} %bitcast.23, bf16[64,1536]{1,0:T(8,128)(2,1)} %bitcast.24, bf16[6,1536]{1,0:T(8,128)(2,1)} %bitcast.27, f32[6]{0:T(128)} %fb_ref.1, s32[16]{0:T(128)} %len_ref.1, ...), custom_call_target="tpu_custom_call" | custom-call | tf_op jit(solution)/shard_map/layer/pallas_call | solution.py:631
  71.4 1.3 %copy.25 = bf16[16,768]{1,0:T(8,128)(2,1)} copy(bf16[16,768]{1,0:T(8,128)(2,1)} %layer.1) | data formatting | bytes 49152
